TPU v7x, 32 devices: a whole 2x2x4 slice. The times are simulated.
32 devices in a mesh: fs: 8 (over z, core), tp: 4 (over y, x).
Axes of the slice: x: 2, y: 2, z: 4, core: 2. Of those that a mesh axis runs over, the one named last changes fastest.
Arguments:
- gate_pre: bfloat16 [8192, 5632], P('fs', 'tp'), may hold values from -6 to 6
- up_pre: bfloat16 [8192, 5632], P('fs', 'tp'), may hold values from -6 to 6
- gate_taps: bfloat16 [3, 5632], replicated, may hold values from -3.5 to 3.5
- up_taps: bfloat16 [3, 5632], replicated, may hold values from -3.5 to 3.5
- down_proj: bfloat16 [5632, 2048], P('tp', 'fs'), may hold values from -0.078125 to 0.078125
- cotangent: bfloat16 [8192, 2048], P(('fs', 'tp')), may hold values from -6 to 6
Outputs:
- gate_grad: bfloat16 [8192, 5632], P('fs', 'tp')
- up_grad: bfloat16 [8192, 5632], P('fs', 'tp')
- down_grad: float32 [5632, 2048], P('tp', 'fs')
- row_norms: float32 [5632], P('tp')
- tap_grads: float32 [2, 3, 5632], replicated
All inputs are finite; a program needn't handle non-finite values.
Results may differ from a plain program's by a relative error of at most 0.0042.
Values may be sent and summed in bfloat16 or wider, within the bound.
A program may use at most 128 MiB of HBM per device.

v0:
```python
import functools
import math

import jax
import jax.numpy as jnp
from jax import lax
from jax.experimental import pallas as pl
from jax.experimental.pallas import tpu as pltpu
from jax.sharding import PartitionSpec as P

MESH = pl.DeviceIdType.MESH


def snake(position, width):
    row, column = position // width, position % width
    return row * width + column + (row % 2) * (width - 1 - 2 * column)


def gather_kernel(chips, tps, cot_ref, down_ref, cot_out, down_out, *sems):
    (ring_send, ring_recv, line_send, line_recv, pair_send, pair_recv, local_sem) = sems
    f, q = lax.axis_index("fs"), lax.axis_index("tp")
    z, core = f // 2, f % 2
    width = math.isqrt(tps)
    spot = snake(q, width)
    half_ring = tps // 2
    ring_next = (snake((spot + 1) % tps, width), snake((spot + tps - 1) % tps, width))
    rows = cot_ref.shape[0]
    cols = down_ref.shape[1]
    partner = z * 2 + 1 - core
    behind, ahead = z > 0, z < chips - 1

    barrier = pltpu.get_barrier_semaphore()
    for device in ({"tp": ring_next[0]}, {"tp": ring_next[1]}, {"fs": partner}):
        pl.semaphore_signal(barrier, inc=1, device_id=device, device_id_type=MESH)

    @pl.when(behind)
    def _():
        pl.semaphore_signal(barrier, inc=1, device_id={"fs": f - 2}, device_id_type=MESH)

    @pl.when(ahead)
    def _():
        pl.semaphore_signal(barrier, inc=1, device_id={"fs": f + 2}, device_id_type=MESH)

    pl.semaphore_wait(barrier, 4 + (z + chips - 1) // chips - (z + 1) // chips)

    def cot_rows(owner_spot, way, part):
        owner = snake((owner_spot + 2 * tps) % tps, width)
        if part:
            return pl.ds(owner * rows + way * (rows // 2), rows // 2)
        return pl.ds(owner * rows, rows)

    def ring_copy(step, way):
        sign = 1 - 2 * way
        part = step == half_ring
        where = cot_rows(spot - sign * (step - 1), way, part)
        if step == 1:
            src = cot_ref.at[pl.ds(way * (rows // 2), rows // 2)] if part else cot_ref
        else:
            src = cot_out.at[where]
        return pltpu.make_async_remote_copy(
            src_ref=src,
            dst_ref=cot_out.at[where],
            send_sem=ring_send.at[way, step - 1],
            recv_sem=ring_recv.at[way, step - 1],
            device_id={"tp": ring_next[way]},
            device_id_type=MESH,
        )

    def ring_landing(step, way):
        sign = 1 - 2 * way
        where = cot_rows(spot - sign * step, way, step == half_ring)
        return pltpu.make_async_remote_copy(
            src_ref=cot_out.at[where],
            dst_ref=cot_out.at[where],
            send_sem=ring_send.at[way, step - 1],
            recv_sem=ring_recv.at[way, step - 1],
            device_id={"tp": ring_next[way]},
            device_id_type=MESH,
        )

    def down_block(chip, which):
        block = chip * 2 + which
        if cols % 128:
            return down_out.at[block]
        return down_out.at[:, pl.ds(pl.multiple_of(block * cols, cols), cols)]

    def line_copy(step, way):
        sign = 1 - 2 * way
        where = down_block(z - sign * (step - 1), core)
        return pltpu.make_async_remote_copy(
            src_ref=down_ref if step == 1 else where,
            dst_ref=where,
            send_sem=line_send.at[way, step - 1],
            recv_sem=line_recv.at[way, step - 1],
            device_id={"fs": f + 2 * sign},
            device_id_type=MESH,
        )

    def line_landing(step, way):
        sign = 1 - 2 * way
        where = down_block(z - sign * step, core)
        return pltpu.make_async_remote_copy(
            src_ref=where,
            dst_ref=where,
            send_sem=line_send.at[way, step - 1],
            recv_sem=line_recv.at[way, step - 1],
            device_id={"fs": f + 2 * sign},
            device_id_type=MESH,
        )

    def pair_copy(step, way, which):
        sign = 1 - 2 * way
        where = down_block(z - sign * step, which)
        slot = step + way * (chips - 1)
        return pltpu.make_async_remote_copy(
            src_ref=down_ref if step == 0 else where,
            dst_ref=where,
            send_sem=pair_send.at[slot],
            recv_sem=pair_recv.at[slot],
            device_id={"fs": partner},
            device_id_type=MESH,
        )

    def has_landing(step, way):
        return z >= step if way == 0 else z + step < chips

    def has_copy(step, way):
        going = ahead if way == 0 else behind
        return going if step == 1 else jnp.logical_and(going, has_landing(step - 1, way))

    for way in range(2):
        ring_copy(1, way).start()

        @pl.when(has_copy(1, way))
        def _():
            line_copy(1, way).start()

    pair_copy(0, 0, core).start()
    own_cot = pltpu.make_async_copy(cot_ref, cot_out.at[pl.ds(q * rows, rows)], local_sem.at[0])
    own_down = pltpu.make_async_copy(down_ref, down_block(z, core), local_sem.at[1])
    own_cot.start()
    own_down.start()

    for step in range(1, max(chips - 1, half_ring) + 1):
        if step <= chips - 1:
            for way in range(2):

                @pl.when(has_landing(step, way))
                def _():
                    line_landing(step, way).wait_recv()
                    pair_copy(step, way, core).start()

                if step + 1 <= chips - 1:

                    @pl.when(has_copy(step + 1, way))
                    def _():
                        line_copy(step + 1, way).start()

        if step <= half_ring:
            for way in range(2):
                ring_landing(step, way).wait_recv()
                if step + 1 <= half_ring:
                    ring_copy(step + 1, way).start()

    own_cot.wait()
    own_down.wait()
    pair_copy(0, 0, 1 - core).wait_recv()
    pair_copy(0, 0, core).wait_send()
    for way in range(2):
        for step in range(1, half_ring + 1):
            ring_copy(step, way).wait_send()
        for step in range(1, chips):

            @pl.when(has_copy(step, way))
            def _():
                line_copy(step, way).wait_send()

            @pl.when(has_landing(step, way))
            def _():
                pair_copy(step, way, 1 - core).wait_recv()
                pair_copy(step, way, core).wait_send()


def gather_both(cotangent, down_proj):
    fs, tps = lax.axis_size("fs"), lax.axis_size("tp")
    chips = fs // 2
    rows, features = cotangent.shape
    channels, cols = down_proj.shape
    dma = pltpu.SemaphoreType.DMA
    down_shape = (fs, channels, cols) if cols % 128 else (channels, cols * fs)
    whole_cot, whole_down = pl.pallas_call(
        functools.partial(gather_kernel, chips, tps),
        out_shape=(
            jax.ShapeDtypeStruct((rows * tps, features), cotangent.dtype),
            jax.ShapeDtypeStruct(down_shape, down_proj.dtype),
        ),
        in_specs=[pl.BlockSpec(memory_space=pltpu.VMEM)] * 2,
        out_specs=[pl.BlockSpec(memory_space=pl.ANY)] * 2,
        scratch_shapes=[
            dma((2, tps // 2)),
            dma((2, tps // 2)),
            dma((2, chips - 1)),
            dma((2, chips - 1)),
            dma((2 * chips - 1,)),
            dma((2 * chips - 1,)),
            dma((2,)),
        ],
        compiler_params=pltpu.CompilerParams(collective_id=0, has_side_effects=True),
        name="gather_both",
    )(cotangent, down_proj)
    if cols % 128:
        whole_down = whole_down.transpose(1, 0, 2).reshape(channels, fs * cols)
    return whole_cot, whole_down


def small_kernel(fs, tps, mine_ref, sum_ref, all_ref, terms, total, sums, *sems):
    send_a, recv_a, send_b, recv_b = sems
    f, q = lax.axis_index("fs"), lax.axis_index("tp")
    barrier = pltpu.get_barrier_semaphore()
    for i in range(1, fs):
        pl.semaphore_signal(
            barrier, inc=1, device_id={"fs": (f + i) % fs}, device_id_type=MESH
        )
    for i in range(1, tps):
        pl.semaphore_signal(
            barrier, inc=1, device_id={"tp": (q + i) % tps}, device_id_type=MESH
        )
    pl.semaphore_wait(barrier, fs + tps - 2)

    def over_fs(i):
        return pltpu.make_async_remote_copy(
            src_ref=mine_ref,
            dst_ref=terms.at[f],
            send_sem=send_a.at[i],
            recv_sem=recv_a.at[i],
            device_id={"fs": (f + i) % fs},
            device_id_type=MESH,
        )

    def over_tp(i):
        return pltpu.make_async_remote_copy(
            src_ref=total,
            dst_ref=sums.at[q],
            send_sem=send_b.at[i],
            recv_sem=recv_b.at[i],
            device_id={"tp": (q + i) % tps},
            device_id_type=MESH,
        )

    def landing(buffer, slot, send, recv, i, device):
        return pltpu.make_async_remote_copy(
            src_ref=buffer.at[slot],
            dst_ref=buffer.at[slot],
            send_sem=send.at[i],
            recv_sem=recv.at[i],
            device_id=device,
            device_id_type=MESH,
        )

    for i in range(1, fs):
        over_fs(i).start()
    terms[f] = mine_ref[...]
    for i in range(1, fs):
        landing(terms, (f + fs - i) % fs, send_a, recv_a, i, {"fs": (f + i) % fs}).wait_recv()
    added = terms[0]
    for i in range(1, fs):
        added = added + terms[i]
    total[...] = added
    sum_ref[...] = added
    sums[q] = added
    for i in range(1, fs):
        over_fs(i).wait_send()
    for i in range(1, tps):
        over_tp(i).start()
    for i in range(1, tps):
        landing(sums, (q + tps - i) % tps, send_b, recv_b, i, {"tp": (q + i) % tps}).wait_recv()
    all_ref[...] = sums[...]
    for i in range(1, tps):
        over_tp(i).wait_send()


def small_sums(mine):
    fs, tps = lax.axis_size("fs"), lax.axis_size("tp")
    dma = pltpu.SemaphoreType.DMA
    shape = mine.shape
    return pl.pallas_call(
        functools.partial(small_kernel, fs, tps),
        out_shape=(
            jax.ShapeDtypeStruct(shape, jnp.float32),
            jax.ShapeDtypeStruct((tps,) + shape, jnp.float32),
        ),
        in_specs=[pl.BlockSpec(memory_space=pltpu.VMEM)],
        out_specs=[pl.BlockSpec(memory_space=pltpu.VMEM)] * 2,
        scratch_shapes=[
            pltpu.VMEM((fs,) + shape, jnp.float32),
            pltpu.VMEM(shape, jnp.float32),
            pltpu.VMEM((tps,) + shape, jnp.float32),
            dma((fs,)),
            dma((fs,)),
            dma((tps,)),
            dma((tps,)),
        ],
        compiler_params=pltpu.CompilerParams(collective_id=1, has_side_effects=True),
        name="small_sums",
    )(mine)


def from_behind(block, axis, distance):
    devices = range(lax.axis_size(axis))
    route = [(i - distance, i) for i in devices if i - distance in devices]
    return lax.ppermute(block, axis, route)


def body(gate_pre, up_pre, gate_taps, up_taps, down_proj, cotangent):
    row_count = gate_pre.shape[0]
    channels = gate_pre.shape[1]
    tap_count = gate_taps.shape[0]
    reach = tap_count - 1
    channel_start = lax.axis_index("tp") * channels
    gate_taps_f = lax.dynamic_slice_in_dim(gate_taps, channel_start, channels, 1).astype(
        jnp.float32
    )
    up_taps_f = lax.dynamic_slice_in_dim(up_taps, channel_start, channels, 1).astype(jnp.float32)
    before = from_behind((gate_pre[row_count - reach :], up_pre[row_count - reach :]), "fs", 1)
    gate_padded = jnp.concatenate([before[0], gate_pre], axis=0).astype(jnp.float32)
    up_padded = jnp.concatenate([before[1], up_pre], axis=0).astype(jnp.float32)
    gate_conv = gate_taps_f[0] * gate_padded[0:row_count]
    up_conv = up_taps_f[0] * up_padded[0:row_count]
    for offset in range(1, tap_count):
        gate_conv = gate_conv + gate_taps_f[offset] * gate_padded[offset : offset + row_count]
        up_conv = up_conv + up_taps_f[offset] * up_padded[offset : offset + row_count]
    gate_sigmoid = jax.nn.sigmoid(gate_conv)
    gate_act = gate_conv * gate_sigmoid
    hidden = (gate_act * up_conv).astype(jnp.bfloat16)
    hidden = lax.optimization_barrier(hidden)
    whole_cot, whole_down = gather_both(cotangent, down_proj)
    grad_scale = 1.0 / math.sqrt(row_count * lax.axis_size("fs"))
    sum_type = jnp.bfloat16 if lax.axis_size("fs") <= 8 else jnp.float32
    terms = lax.dot_general(
        whole_cot, hidden, (((0,), (0,)), ((), ())), preferred_element_type=jnp.float32
    ).astype(sum_type)
    terms, whole_down = lax.optimization_barrier((terms, whole_down))
    own_rows = lax.psum_scatter(terms, "fs", scatter_dimension=0, tiled=True)
    own_rows = own_rows.astype(jnp.float32) * grad_scale
    hidden_grad = lax.dot_general(
        whole_cot,
        whole_down,
        (((1,), (1,)), ((), ())),
        preferred_element_type=jnp.float32,
    )
    gate_conv_grad = hidden_grad * up_conv * gate_sigmoid * (1.0 + gate_conv * (1.0 - gate_sigmoid))
    up_conv_grad = hidden_grad * gate_act
    following = from_behind((gate_conv_grad[0:reach], up_conv_grad[0:reach]), "fs", -1)
    gate_grad_pad = jnp.concatenate([gate_conv_grad, following[0]], axis=0)
    up_grad_pad = jnp.concatenate([up_conv_grad, following[1]], axis=0)
    gate_grad = gate_taps_f[0] * gate_grad_pad[reach : reach + row_count]
    up_grad = up_taps_f[0] * up_grad_pad[reach : reach + row_count]
    for offset in range(1, tap_count):
        lead = reach - offset
        gate_grad = gate_grad + gate_taps_f[offset] * gate_grad_pad[lead : lead + row_count]
        up_grad = up_grad + up_taps_f[offset] * up_grad_pad[lead : lead + row_count]
    gate_tap_terms = jnp.stack(
        [
            jnp.sum(gate_conv_grad * gate_padded[offset : offset + row_count], axis=0)
            for offset in range(tap_count)
        ]
    )
    up_tap_terms = jnp.stack(
        [
            jnp.sum(up_conv_grad * up_padded[offset : offset + row_count], axis=0)
            for offset in range(tap_count)
        ]
    )
    tap_terms = jnp.stack([gate_tap_terms, up_tap_terms])
    feature_count = whole_cot.shape[1]
    down_grad = own_rows.T
    partial_norms = jnp.sum(own_rows * own_rows, axis=0)
    tap_rows = tap_terms.reshape(2 * tap_count, channels)
    pad = -(2 * tap_count + 1) % 8
    mine = jnp.concatenate(
        [tap_rows, partial_norms[None], jnp.zeros((pad, channels), jnp.float32)], axis=0
    )
    summed, everywhere = small_sums(mine)
    row_norms = summed[2 * tap_count] / feature_count
    tap_grads = (
        everywhere[:, : 2 * tap_count].transpose(1, 0, 2).reshape(2, tap_count, -1) * grad_scale
    )
    return (
        gate_grad.astype(jnp.bfloat16),
        up_grad.astype(jnp.bfloat16),
        down_grad,
        row_norms,
        tap_grads,
    )


def solution(mesh):
    placed = (P("fs", "tp"), P("fs", "tp"), P(), P(), P("tp", "fs"), P(("fs", "tp"), None))
    return jax.shard_map(
        body,
        mesh=mesh,
        in_specs=placed,
        out_specs=(P("fs", "tp"), P("fs", "tp"), P("tp", "fs"), P("tp"), P()),
        check_vma=False,
    )
```

profile of v0, /device:TPU:0, one launch (start us, length us, event | category | flops | bytes accessed | tf_op | source)
XLA Modules:
  0.0 196.4 jit_solution(6308761135780003241)
XLA Ops:
  7.2 0.7 slice.79
  8.0 2.4 %collective-permute-start = (bf16[2,1408]{1,0:T(2,128)(2,1)S(1)}, bf16[2,1408]{1,0:T(2,128)(2,1)S(1)}, u32[]{:S(2)}, u32[]{:S(2)}) collective-permute-start(bf16[2,1408]{1,0:T(2,128)(2,1)S(1)} %slice.79), channel_id=1, source_target_pairs={{0,4},{4,8},{8,12},{12,16},{16,20},{20,24},{24,28},{1,5},{5,9},{9,... | collective-permute-start | bytes 16904 | tf_op jit(solution)/shard_map/ppermute | solution.py:311
  10.4 0.7 slice.86
  11.1 4.6 %collective-permute-start.1 = (bf16[2,1408]{1,0:T(2,128)(2,1)S(1)}, bf16[2,1408]{1,0:T(2,128)(2,1)S(1)}, u32[]{:S(2)}, u32[]{:S(2)}) collective-permute-start(bf16[2,1408]{1,0:T(2,128)(2,1)S(1)} %slice.86), channel_id=1, source_target_pairs={{0,4},{4,8},{8,12},{12,16},{16,20},{20,24},{24,28},{1,5},{5,9},{9,... | collective-permute-start | bytes 16904 | tf_op jit(solution)/shard_map/ppermute | solution.py:311
  15.7 0.7 dynamic-slice_convert_fusion
  16.5 56.2 %gather_both.1 = (bf16[1024,2048]{1,0:T(8,128)(2,1)}, bf16[1408,2048]{1,0:T(8,128)(2,1)}) custom-call(bf16[256,2048]{1,0:T(8,128)(2,1)} %cot_ref.1, bf16[1408,256]{1,0:T(8,128)(2,1)} %down_ref.1), custom_call_target="tpu_custom_call" | custom-call | tf_op jit(solution)/shard_map/gather_both/pallas_call | solution.py:191
  72.8 2.5 %maximum_convert_fusion = f32[1026,1408]{1,0:T(8,128)S(1)} fusion(bf16[1024,1408]{1,0:T(8,128)(2,1)} %param.6, bf16[2,1408]{1,0:T(2,128)(2,1)S(1)} %collective-permute-done), kind=kLoop, calls=%fused_computation.31 | loop fusion | flops 5778432 | bytes 8667648 | tf_op jit(solution)/shard_map/convert_element_type | solution.py:325
  75.4 3.5 %maximum_convert_fusion.1 = f32[1026,1408]{1,0:T(8,128)} fusion(bf16[1024,1408]{1,0:T(8,128)(2,1)S(1)} %copy-done.2, bf16[2,1408]{1,0:T(2,128)(2,1)S(1)} %collective-permute-done.1), kind=kLoop, calls=%fused_computation.32 | loop fusion | flops 5778432 | bytes 8667648 | tf_op jit(solution)/shard_map/convert_element_type | solution.py:326
  78.9 12.8 %multiply_convert_fusion = (bf16[1024,1408]{1,0:T(8,128)(2,1)}, f32[1024,1408]{1,0:T(8,128)}, f32[1024,1408]{1,0:T(8,128)}) fusion(f32[1026,1408]{1,0:T(8,128)} %maximum_convert_fusion.1, f32[1408]{0:T(1024)S(1)} %get-tuple-element.34, f32[1408]{0:T(1024)S(1)} %get-tuple-element.35, f32[1408]{0:T(1024)S(1)} %get-tuple-element.33, ...), kind=kLoop, calls=%fused_computation.26 | loop fusion | flops 23068672 | bytes 49054720 | tf_op jit(solution)/shard_map/convert_element_type | solution.py:334
  91.7 10.9 %convolution_convert_fusion = bf16[2048,1408]{1,0:T(8,128)(2,1)} fusion(bf16[1024,2048]{1,0:T(8,128)(2,1)} %get-tuple-element.11, bf16[1024,1408]{1,0:T(8,128)(2,1)} %get-tuple-element.41), kind=kOutput, calls=%fused_computation | convolution fusion | flops 5908463616 | bytes 12845056 | tf_op jit(solution)/shard_map/dot_general | solution.py:339
  102.8 11.9 %fusion.16 = f32[1024,1408]{1,0:T(8,128)} fusion(bf16[1024,2048]{1,0:T(8,128)(2,1)} %get-tuple-element.11, bf16[1408,2048]{1,0:T(8,128)(2,1)} %get-tuple-element.13), kind=kOutput, calls=%fused_computation.51 | convolution fusion | flops 5905580032 | bytes 15728640 | tf_op jit(solution)/shard_map/dot_general | solution.py:345
  114.7 14.5 %multiply_reduce_fusion.2 = (f32[1408]{0:T(1024)S(1)}, f32[1408]{0:T(1024)S(1)}, f32[1408]{0:T(1024)S(1)}, f32[1024,1408]{1,0:T(8,128)}, f32[1408]{0:T(1024)S(1)...) fusion(f32[1026,1408]{1,0:T(8,128)S(1)} %bitcast.16, f32[1024,1408]{1,0:T(8,128)} %fusion.16, ...), kind=kLoop, calls=%fused_computation.21 | loop fusion | flops 33152768 | bytes 63472640 | tf_op jit(solution)/shard_map/reduce_sum | solution.py:370
  129.2 0.8 slice.115
  130.0 1.3 collective-permute-start.3
  131.4 0.9 slice.112
  132.4 1.5 collective-permute-start.2
  133.9 11.6 %fusion.4 = bf16[1024,1408]{1,0:T(8,128)(2,1)} fusion(f32[1024,1408]{1,0:T(8,128)} %get-tuple-element.40, f32[2,1408]{1,0:T(2,128)S(1)} %collective-permute-done.3, f32[1408]{0:T(1024)S(1)} %get-tuple-element.34, f32[1408]{0:T(1024)S(1)} %get-tuple-element.35, f32[1408]{0:T(1024)S(1)} %get-tuple-element.33), kind=kLoop, calls=%fused_computation.9 | loop fusion | flops 11534336 | bytes 8678912 | tf_op jit(solution)/shard_map/convert_element_type | solution.py:390
  145.5 5.3 %fusion.9 = bf16[1024,1408]{1,0:T(8,128)(2,1)} fusion(f32[1024,1408]{1,0:T(8,128)S(1)} %copy-done.1, f32[2,1408]{1,0:T(2,128)S(1)} %collective-permute-done.2, f32[1408]{0:T(1024)S(1)} %get-tuple-element.37, f32[1408]{0:T(1024)S(1)} %get-tuple-element.38, f32[1408]{0:T(1024)S(1)} %get-tuple-element.36), kind=kLoop, calls=%fused_computation.14 | loop fusion | flops 11534336 | bytes 8678912 | tf_op jit(solution)/shard_map/convert_element_type | solution.py:389
  150.9 16.0 %reduce-scatter.2.cloned.1.call-done = bf16[256,1408]{1,0:T(8,128)(2,1)} async-done(((bf16[2048,1408]{1,0:T(8,128)(2,1)}), bf16[256,1408]{1,0:T(8,128)(2,1)}) %reduce-scatter.2.cloned.1.call-update) | async-done | bytes 720912 | tf_op jit(solution)/shard_map/reduce_scatter | solution.py:343
  166.8 1.3 multiply_reduce_fusion.6
  168.9 15.9 %small_sums.1 = (f32[8,1408]{1,0:T(8,128)}, f32[4,8,1408]{2,1,0:T(8,128)}) custom-call(f32[8,1408]{1,0:T(8,128)} %maximum_maximum_fusion.mine_ref), custom_call_target="tpu_custom_call" | custom-call | tf_op jit(solution)/shard_map/small_sums/pallas_call | solution.py:286
  184.8 0.9 multiply_bitcast_fusion
  186.6 1.4 multiply_reduce_fusion.7
  188.0 1.5 copy.13
  (40 shorter events, 2.0 us)
Async XLA Ops:
  7.2 159.7 %reduce-scatter.2.cloned.1.call-start = ((), (), s32[]{:S(2)}) async-start(), calls=%async_computation.1 | async-start | bytes 6488064 | tf_op jit(solution)/shard_map/reduce_scatter | solution.py:343
  8.0 64.8 %collective-permute-start = (bf16[2,1408]{1,0:T(2,128)(2,1)S(1)}, bf16[2,1408]{1,0:T(2,128)(2,1)S(1)}, u32[]{:S(2)}, u32[]{:S(2)}) collective-permute-start(bf16[2,1408]{1,0:T(2,128)(2,1)S(1)} %slice.79), channel_id=1, source_target_pairs={{0,4},{4,8},{8,12},{12,16},{16,20},{20,24},{24,28},{1,5},{5,9},{9,... | collective-permute-start | bytes 16904 | tf_op jit(solution)/shard_map/ppermute | solution.py:311
  11.1 64.2 %collective-permute-start.1 = (bf16[2,1408]{1,0:T(2,128)(2,1)S(1)}, bf16[2,1408]{1,0:T(2,128)(2,1)S(1)}, u32[]{:S(2)}, u32[]{:S(2)}) collective-permute-start(bf16[2,1408]{1,0:T(2,128)(2,1)S(1)} %slice.86), channel_id=1, source_target_pairs={{0,4},{4,8},{8,12},{12,16},{16,20},{20,24},{24,28},{1,5},{5,9},{9,... | collective-permute-start | bytes 16904 | tf_op jit(solution)/shard_map/ppermute | solution.py:311
  72.8 2.7 %copy-start.2 = (bf16[1024,1408]{1,0:T(8,128)(2,1)S(1)}, bf16[1024,1408]{1,0:T(8,128)(2,1)}, u32[]{:S(2)}) copy-start(bf16[1024,1408]{1,0:T(8,128)(2,1)} %param.7) | copy-start | bytes 8650756
  75.3 16.4 %copy-start = (f32[1026,1408]{1,0:T(8,128)}, f32[1026,1408]{1,0:T(8,128)S(1)}, u32[]{:S(2)}) copy-start(f32[1026,1408]{1,0:T(8,128)S(1)} %maximum_convert_fusion) | copy-start | bytes 17335300
  102.7 12.0 %slice-start = ((s8[5812224]{0:T(1024)(128)(4,1)}), s8[4194304]{0:T(1024)(128)(4,1)S(1)}, s32[]{:S(2)}) async-start(s8[5812224]{0:T(1024)(128)(4,1)} %bitcast.13), calls=%async_computation.2 | async-start | bytes 8388608
  102.7 12.0 %slice-start.2 = ((s8[5812224]{0:T(1024)(128)(4,1)}), s8[4194304]{0:T(1024)(128)(4,1)S(1)}, s32[]{:S(2)}) async-start(s8[5812224]{0:T(1024)(128)(4,1)} %bitcast.15), calls=%async_computation.4 | async-start | bytes 8388608
  102.7 11.9 %slice-start.1 = ((s8[5812224]{0:T(1024)(128)(4,1)}), s8[1617920]{0:T(1024)(128)(4,1)S(1)}, s32[]{:S(2)}) async-start(s8[5812224]{0:T(1024)(128)(4,1)} %bitcast.13), calls=%async_computation.3 | async-start | bytes 3235840
  102.8 11.9 %slice-start.3 = ((s8[5812224]{0:T(1024)(128)(4,1)}), s8[1617920]{0:T(1024)(128)(4,1)S(1)}, s32[]{:S(2)}) async-start(s8[5812224]{0:T(1024)(128)(4,1)} %bitcast.15), calls=%async_computation.5 | async-start | bytes 3235840
  130.0 3.9 %collective-permute-start.3 = (f32[2,1408]{1,0:T(2,128)S(1)}, f32[2,1408]{1,0:T(2,128)S(1)}, u32[]{:S(2)}, u32[]{:S(2)}) collective-permute-start(f32[2,1408]{1,0:T(2,128)S(1)} %slice.115), channel_id=1, source_target_pairs={{4,0},{8,4},{12,8},{16,12},{20,16},{24,20},{28,24},{5,1},{9,5},{13... | collective-permute-start | bytes 33800 | tf_op jit(solution)/shard_map/ppermute | solution.py:311
  131.4 14.1 %copy-start.1 = (f32[1024,1408]{1,0:T(8,128)S(1)}, f32[1024,1408]{1,0:T(8,128)}, u32[]{:S(2)}) copy-start(f32[1024,1408]{1,0:T(8,128)} %get-tuple-element.47) | copy-start | bytes 17301508
  132.4 13.2 %collective-permute-start.2 = (f32[2,1408]{1,0:T(2,128)S(1)}, f32[2,1408]{1,0:T(2,128)S(1)}, u32[]{:S(2)}, u32[]{:S(2)}) collective-permute-start(f32[2,1408]{1,0:T(2,128)S(1)} %slice.112), channel_id=1, source_target_pairs={{4,0},{8,4},{12,8},{16,12},{20,16},{24,20},{28,24},{5,1},{9,5},{13... | collective-permute-start | bytes 33800 | tf_op jit(solution)/shard_map/ppermute | solution.py:311
Sparse Core Ops, SparseCore 0:
  102.8 64.0 reduce-scatter.1
where the time goes:
time: 197 us; the launch traced here: 196 us
  Pallas kernels  72.1 us (37%)
  other arithmetic  55.3 us (28%)
  matrix products  22.8 us (12%)
  waiting for transfers between devices  16 us (8%)
  between operations  14.3 us (7%)
  starting transfers between devices  9.84 us (5%)
  local copies, waits for them, and re-layouts  5.98 us (3%)
    pallas_call x1, Pallas kernels, gather_both(): pl.pallas_call(functools.partial(gather_kernel, chips, tps), out_shape=(j...  56.2 us
    reduce_scatter x1, waiting for transfers between devices, body(): own_rows = lax.psum_scatter(terms, 'fs', scatter_dimension=0, tiled=True)  16 us
    pallas_call x1, Pallas kernels, small_sums(): pl.pallas_call(functools.partial(small_kernel, fs, tps), out_shape=(jax.S...  15.9 us
    reduce_sum x1, other arithmetic, body(): jnp.sum(up_conv_grad * up_padded[offset:offset + row_count], axis=0)  14.5 us
    convert_element_type x1, other arithmetic, body(): hidden = (gate_act * up_conv).astype(jnp.bfloat16)  12.8 us
    dot_general x1, matrix products, body(): lax.dot_general(whole_cot, whole_down, (((1,), (1,)), ((), ())), preferre...  11.9 us
    convert_element_type x1, other arithmetic, body(): up_grad.astype(jnp.bfloat16)  11.6 us
    dot_general x1, matrix products, body(): lax.dot_general(whole_cot, hidden, (((0,), (0,)), ((), ())), preferred_el...  10.9 us
  transfers between devices with their start and end apart: 5, of which 1 were waited for; matrix products, arithmetic and copies ran while one was open for 25% of the time, Pallas kernels for 29%

commit v1 on v0

--- a/solution.py
+++ b/solution.py
@@ -311,7 +311,7 @@
     return lax.ppermute(block, axis, route)
 
 
-def body(gate_pre, up_pre, gate_taps, up_taps, down_proj, cotangent):
+def staged_body(gate_pre, up_pre, gate_taps, up_taps, down_proj, cotangent):
     row_count = gate_pre.shape[0]
     channels = gate_pre.shape[1]
     tap_count = gate_taps.shape[0]
@@ -394,6 +394,765 @@
     )
 
 
+PIECES = 2
+ROW_TILE = 128
+SUB = 32
+BLOCK = 64
+LANES = 128
+BF16_ROWS = 16
+
+
+def less(a, b):
+    return (b - a - 1 + 4096) // 4096
+
+
+def whole_kernel(
+    chips,
+    tps,
+    scale,
+    gate_ref,
+    up_ref,
+    gtaps_ref,
+    utaps_ref,
+    down_ref,
+    cot_ref,
+    gate_out,
+    up_out,
+    down_out,
+    norm_out,
+    taps_out,
+    gate_v,
+    up_v,
+    taps_v,
+    a_v,
+    b_v,
+    hid_t,
+    cot_v,
+    down_v,
+    pair_send,
+    pair_recv,
+    rs_recv,
+    rs_send,
+    dg_v,
+    hg_v,
+    edge_send,
+    edge_recv,
+    acc_v,
+    tap_mine,
+    tap_pair,
+    tap_chip,
+    tap_all,
+    norm_all,
+    *sems,
+):
+    (local, z_send, z_recv, pd_send, pd_recv, pt_send, pt_recv, c_send, c_recv) = sems[:9]
+    (h_send, h_recv, e_send, e_recv, tp_send, tp_recv, tz_send, tz_recv) = sems[9:17]
+    (ta_send, ta_recv, tb_send, tb_recv, n_send, n_recv) = sems[17:]
+    f, q = lax.axis_index("fs"), lax.axis_index("tp")
+    z, core = f // 2, f % 2
+    fs = 2 * chips
+    partner = z * 2 + 1 - core
+    rows, features = cot_ref.shape
+    channels, cols = down_ref.shape
+    total_rows = rows * tps
+    chip_cols = 2 * cols
+    piece = channels // PIECES
+    lane_tiles = channels // LANES
+    half = z // (chips // 2)
+    width = math.isqrt(tps)
+    spot = snake(q, width)
+    half_ring = tps // 2
+    ring_next = (snake((spot + 1) % tps, width), snake((spot + tps - 1) % tps, width))
+    f32, bf16 = jnp.float32, jnp.bfloat16
+
+    def remote(src, dst, send, recv, device):
+        return pltpu.make_async_remote_copy(
+            src_ref=src,
+            dst_ref=dst,
+            send_sem=send,
+            recv_sem=recv,
+            device_id=device,
+            device_id_type=MESH,
+        )
+
+    def down_piece(chip, which, s):
+        col = pl.multiple_of(chip * chip_cols + which * cols, cols)
+        return down_v.at[pl.ds(s * piece, piece), pl.ds(col, cols)]
+
+    own_cot = pltpu.make_async_copy(
+        cot_ref, cot_v.at[pl.ds(pl.multiple_of(q * rows, rows), rows)], local.at[0]
+    )
+    own_down = pltpu.make_async_copy(
+        down_ref,
+        down_v.at[:, pl.ds(pl.multiple_of(f * cols, cols), cols)],
+        local.at[1],
+    )
+    load_gate = pltpu.make_async_copy(
+        gate_ref, gate_v.at[pl.ds(BF16_ROWS, total_rows)], local.at[2]
+    )
+    load_up = pltpu.make_async_copy(up_ref, up_v.at[pl.ds(BF16_ROWS, total_rows)], local.at[3])
+    own_down.start()
+    own_cot.start()
+    load_gate.start()
+    load_up.start()
+
+    barrier = pltpu.get_barrier_semaphore()
+    for i in range(1, fs):
+        pl.semaphore_signal(barrier, inc=1, device_id={"fs": (f + i) % fs}, device_id_type=MESH)
+    for i in range(1, tps):
+        pl.semaphore_signal(barrier, inc=1, device_id={"tp": (q + i) % tps}, device_id_type=MESH)
+    pl.semaphore_wait(barrier, fs + tps - 2)
+
+    def chip_at(position, way):
+        return position + way * (chips - 1 - 2 * position)
+
+    def z_copy(src, dst, way, p, s):
+        return remote(
+            src,
+            dst,
+            z_send.at[way, p, s],
+            z_recv.at[way, p, s],
+            {"fs": (f + 2 * (1 - 2 * way) + fs) % fs},
+        )
+
+    def pair_down(chip, which, s):
+        where = down_piece(chip, which, s)
+        return remote(where, where, pd_send.at[chip, s], pd_recv.at[chip, s], {"fs": partner})
+
+    def halo_copy(i, src, dst):
+        return remote(
+            src.at[pl.ds(total_rows - BF16_ROWS, BF16_ROWS)],
+            dst.at[pl.ds(0, BF16_ROWS)],
+            h_send.at[i],
+            h_recv.at[i],
+            {"fs": (f + 1) % fs},
+        )
+
+    def chunk_chip(k):
+        near = z + half * (chips - 1 - 2 * z)
+        if k == chips - 1:
+            position = near
+        else:
+            far = chips - 1 - near
+            first = less(k, far)
+            position = first * (chips - 1 - k) + (1 - first) * (k - far)
+        return position + half * (chips - 1 - 2 * position)
+
+    def cot_part(owner_spot, way, part, k):
+        owner = snake((owner_spot + 2 * tps) % tps, width)
+        col = pl.ds(pl.multiple_of(chunk_chip(k) * chip_cols, chip_cols), chip_cols)
+        if part:
+            start = owner * rows + way * (rows // 2)
+            return cot_v.at[pl.ds(pl.multiple_of(start, rows // 2), rows // 2), col]
+        return cot_v.at[pl.ds(pl.multiple_of(owner * rows, rows), rows), col]
+
+    def ring_copy(k, step, way):
+        sign = 1 - 2 * way
+        where = cot_part(spot - sign * (step - 1), way, step == half_ring, k)
+        return remote(
+            where,
+            where,
+            c_send.at[k, way, step - 1],
+            c_recv.at[k, way, step - 1],
+            {"tp": ring_next[way]},
+        )
+
+    def ring_landing(k, step, way):
+        sign = 1 - 2 * way
+        where = cot_part(spot - sign * step, way, step == half_ring, k)
+        return remote(
+            where,
+            where,
+            c_send.at[k, way, step - 1],
+            c_recv.at[k, way, step - 1],
+            {"tp": ring_next[way]},
+        )
+
+    def ring_step(k, step):
+        for way in range(2):
+            ring_landing(k, step, way).wait_recv()
+            if step < half_ring:
+                ring_copy(k, step + 1, way).start()
+        if step == 1:
+            for ahead in range(1 + min(k, 1), 3):
+                if k + ahead < chips:
+                    for way in range(2):
+                        ring_copy(k + ahead, 1, way).start()
+
+    own_down.wait()
+
+    @pl.when(f < fs - 1)
+    def _():
+        halo_copy(0, gate_ref, gate_v).start()
+        halo_copy(1, up_ref, up_v).start()
+
+    for s in range(PIECES):
+        where = down_piece(z, core, s)
+
+        @pl.when(z < chips - 1)
+        def _():
+            z_copy(where, where, 0, 0, s).start()
+
+        @pl.when(z > 0)
+        def _():
+            z_copy(where, where, 1, 0, s).start()
+
+    own_cot.wait()
+    for way in range(2):
+        ring_copy(0, 1, way).start()
+    for s in range(PIECES):
+        pair_down(z, core, s).start()
+
+    tap_col = pl.multiple_of(q * channels, LANES)
+    taps_v[0, 0:3, :] = gtaps_ref[:, pl.ds(tap_col, channels)].astype(f32)
+    taps_v[1, 0:3, :] = utaps_ref[:, pl.ds(tap_col, channels)].astype(f32)
+
+    def hidden_tile(tile, lane_tile):
+        lane = pl.ds(pl.multiple_of(lane_tile * LANES, LANES), LANES)
+        gt = [taps_v[0, k : k + 1, lane] for k in range(3)]
+        ut = [taps_v[1, k : k + 1, lane] for k in range(3)]
+        parts = []
+        for i in range(ROW_TILE // SUB):
+            start = pl.multiple_of(tile * ROW_TILE + i * SUB, SUB)
+            window = pl.ds(start, SUB + BF16_ROWS)
+            g = gate_v[window, lane].astype(f32)
+            u = up_v[window, lane].astype(f32)
+            g_conv = (
+                gt[0] * pltpu.roll(g, 2, 0)[BF16_ROWS:]
+                + gt[1] * pltpu.roll(g, 1, 0)[BF16_ROWS:]
+                + gt[2] * g[BF16_ROWS:]
+            )
+            u_conv = (
+                ut[0] * pltpu.roll(u, 2, 0)[BF16_ROWS:]
+                + ut[1] * pltpu.roll(u, 1, 0)[BF16_ROWS:]
+                + ut[2] * u[BF16_ROWS:]
+            )
+            sig = 0.5 * jnp.tanh(0.5 * g_conv) + 0.5
+            act = g_conv * sig
+            out = pl.ds(start, SUB)
+            a_v[out, lane] = u_conv * (sig + act * (1.0 - sig))
+            b_v[out, lane] = act
+            parts.append((act * u_conv).astype(bf16))
+        tile_t = jnp.concatenate(parts, axis=0).T
+        hid_t[lane, pl.ds(pl.multiple_of(tile * ROW_TILE, ROW_TILE), ROW_TILE)] = tile_t
+
+    def hidden_tiles(first, count):
+        def step(i, carry):
+            hidden_tile(first + i // lane_tiles, i % lane_tiles)
+            return carry
+
+        lax.fori_loop(0, count * lane_tiles, step, 0)
+
+    tiles = total_rows // ROW_TILE
+    load_gate.wait()
+    load_up.wait()
+    hidden_tiles(tiles // 2, tiles - tiles // 2)
+    ring_step(0, 1)
+    hidden_tiles(1, tiles // 2 - 1)
+
+    @pl.when(f > 0)
+    def _():
+        halo_copy(0, gate_ref, gate_v).wait_recv()
+        halo_copy(1, up_ref, up_v).wait_recv()
+
+    @pl.when(f == 0)
+    def _():
+        gate_v[0:BF16_ROWS, :] = jnp.zeros((BF16_ROWS, channels), bf16)
+        up_v[0:BF16_ROWS, :] = jnp.zeros((BF16_ROWS, channels), bf16)
+
+    hidden_tiles(0, 1)
+
+    def terms(s, chip, which):
+        col = pl.multiple_of(chip * chip_cols + which * cols, cols)
+        return jnp.dot(
+            hid_t[pl.ds(pl.multiple_of(s * piece, BF16_ROWS), piece), :],
+            cot_v[:, pl.ds(col, cols)],
+            preferred_element_type=f32,
+        )
+
+    def pair_terms_copy(chip):
+        return remote(
+            pair_send.at[chip],
+            pair_recv.at[chip],
+            pt_send.at[chip],
+            pt_recv.at[chip],
+            {"fs": partner},
+        )
+
+    def pair_terms(k):
+        chip = chunk_chip(k)
+
+        def step(s, carry):
+            here = pl.ds(pl.multiple_of(s * piece, BF16_ROWS), piece)
+            pair_send[chip, here, :] = terms(s, chip, 1 - core).astype(bf16)
+            return carry
+
+        lax.fori_loop(0, PIECES, step, 0)
+        pair_terms_copy(chip).start()
+
+    def pair_terms_wait(k):
+        pair_terms_copy(chunk_chip(k)).wait_recv()
+
+    def send_sum(position, way, p, s, first):
+        chip = chip_at(chips - 1 + position - p, way)
+        here = pl.ds(s * piece, piece)
+        value = terms(s, chip, core) + pair_recv[chip, here, :].astype(f32)
+        if not first:
+            earlier = rs_recv[way, chip, here, :].astype(f32)
+            value = value + jnp.where(position > 0, earlier, 0.0)
+        rs_send[chip, here, :] = value.astype(bf16)
+        z_copy(rs_send.at[chip, here], rs_recv.at[way, chip, here], way, p + 1, s).start()
+
+    def both_ways(body):
+        def step(d, carry):
+            way = (half + d) % 2
+            body(way, z + way * (chips - 1 - 2 * z))
+            return carry
+
+        lax.fori_loop(0, 2, step, 0)
+
+    def first_sums():
+        def body(way, position):
+            @pl.when(position == 0)
+            def _():
+                for s in range(PIECES):
+                    send_sum(position, way, 0, s, True)
+
+        both_ways(body)
+
+    def slot(p, s):
+        here = pl.ds(s * piece, piece)
+
+        def body(way, position):
+            @pl.when(position > p)
+            def _():
+                chip = chip_at(position - 1 - p, way)
+                where = down_piece(chip, core, s)
+                z_copy(where, where, way, p, s).wait_recv()
+                if p + 1 < chips:
+
+                    @pl.when(position < chips - 1)
+                    def _():
+                        z_copy(where, where, way, p + 1, s).start()
+
+                pair_down(chip, core, s).start()
+
+            if p > 0:
+
+                @pl.when(jnp.logical_and(position > 0, position <= p))
+                def _():
+                    chip = chip_at(chips - 1 + position - p, way)
+                    where = rs_recv.at[way, chip, here]
+                    z_copy(where, where, way, p, s).wait_recv()
+
+                if p + 1 < chips:
+
+                    @pl.when(position <= p)
+                    def _():
+                        send_sum(position, way, p, s, False)
+
+        both_ways(body)
+
+    def pair_down_wait(chip):
+        for s in range(PIECES):
+            pair_down(chip, 1 - core, s).wait_recv()
+
+    last_chip = (1 - half) * (chips - 1)
+
+    def hidden_grad(first_chip, count, add):
+        depth = count * chip_cols
+        col = pl.ds(pl.multiple_of(first_chip * chip_cols, chip_cols), depth)
+
+        def one(start, size):
+            lane = pl.ds(start, size)
+            value = lax.dot_general(
+                cot_v[:, col],
+                down_v[lane, col],
+                (((1,), (1,)), ((), ())),
+                preferred_element_type=f32,
+            )
+            if add:
+                value = value + hg_v[0:total_rows, lane]
+            hg_v[0:total_rows, lane] = value
+
+        wide = 2 * LANES
+
+        def step(n, carry):
+            one(pl.multiple_of(n * wide, wide), wide)
+            return carry
+
+        lax.fori_loop(0, channels // wide, step, 0)
+        if channels % wide:
+            one(channels - channels % wide, channels % wide)
+
+    slot(0, 0)
+    for step in range(2, half_ring + 1):
+        ring_step(0, step)
+    pair_terms(0)
+    pair_terms_wait(0)
+    first_sums()
+    for s in range(1, PIECES):
+        slot(0, s)
+    ring_step(1, 1)
+    for p in range(1, chips - 1):
+        ring_step(p + 1, 1)
+        for step in range(2, half_ring + 1):
+            ring_step(p, step)
+        pair_terms(p)
+        pair_terms_wait(p)
+        if p < chips - 2:
+            for s in range(PIECES):
+                slot(p, s)
+    for step in range(2, half_ring + 1):
+        ring_step(chips - 1, step)
+    pair_terms(chips - 1)
+    slot(chips - 2, 0)
+    for i in range(chips - 1):
+        pair_down_wait(half + i)
+    hidden_grad(half, chips - 1, False)
+    pair_terms_wait(chips - 1)
+    for s in range(1, PIECES):
+        slot(chips - 2, s)
+
+    def own_terms(s, carry):
+        here = pl.ds(pl.multiple_of(s * piece, BF16_ROWS), piece)
+        dg_v[here, :] = terms(s, z, core) + pair_recv[z, here, :].astype(f32)
+        return carry
+
+    lax.fori_loop(0, PIECES, own_terms, 0)
+    pair_down_wait(last_chip)
+    hidden_grad(last_chip, 1, True)
+
+    edge = 8
+    row_index = lax.broadcasted_iota(jnp.int32, (edge, channels), 0)
+    top = pl.ds(0, edge)
+    edge_send[...] = jnp.where(
+        row_index < 2,
+        hg_v[top, :] * a_v[top, :],
+        pltpu.roll(hg_v[top, :] * b_v[top, :], 2, 0),
+    )
+    edge_copy = remote(
+        edge_send, edge_recv, e_send.at[0], e_recv.at[0], {"fs": (f + fs - 1) % fs}
+    )
+
+    @pl.when(f > 0)
+    def _():
+        edge_copy.start()
+
+    def grads(start, lane, sums):
+        window = pl.ds(start, BLOCK + edge)
+        here = pl.ds(pl.multiple_of(start + BF16_ROWS, BF16_ROWS), BLOCK)
+        hg = hg_v[window, lane]
+        new = []
+        for b, (factor, pre) in enumerate(((a_v, gate_v), (b_v, up_v))):
+            g = hg * factor[window, lane]
+            g0 = g[0:BLOCK]
+            g1 = pltpu.roll(g, BLOCK + edge - 1, 0)[0:BLOCK]
+            g2 = pltpu.roll(g, BLOCK + edge - 2, 0)[0:BLOCK]
+            x = pre[here, lane].astype(f32)
+            for i, shifted in enumerate((g2, g1, g0)):
+                product = (shifted * x).reshape(BLOCK // 8, 8, LANES)
+                new.append(sums[3 * b + i] + jnp.sum(product, axis=0))
+            t = [taps_v[b, k : k + 1, lane] for k in range(3)]
+            pre[here, lane] = (t[0] * g2 + t[1] * g1 + t[2] * g0).astype(bf16)
+        return tuple(new)
+
+    blocks = total_rows // BLOCK
+
+    def grad_lanes(lane_tile, carry):
+        lane = pl.ds(pl.multiple_of(lane_tile * LANES, LANES), LANES)
+
+        def step(i, sums):
+            return grads(pl.multiple_of(i * BLOCK, BLOCK), lane, sums)
+
+        zero = jnp.zeros((8, LANES), f32)
+        sums = lax.fori_loop(0, blocks - 1, step, (zero,) * 6)
+        for i in range(6):
+            acc_v[i, :, lane] = sums[i]
+        return carry
+
+    def grad_last(lane_tile, carry):
+        lane = pl.ds(pl.multiple_of(lane_tile * LANES, LANES), LANES)
+        sums = grads((blocks - 1) * BLOCK, lane, tuple(acc_v[i, :, lane] for i in range(6)))
+        for b in range(2):
+            for k in range(3):
+                tap_mine[b, k : k + 1, lane] = jnp.sum(sums[3 * b + k], axis=0, keepdims=True)
+        return carry
+
+    lax.fori_loop(0, lane_tiles // 2, grad_lanes, 0)
+    lax.fori_loop(lane_tiles // 2, lane_tiles, grad_lanes, 0)
+
+    @pl.when(f < fs - 1)
+    def _():
+        edge_copy.wait_recv()
+
+    @pl.when(f == fs - 1)
+    def _():
+        edge_recv[...] = jnp.zeros((edge, channels), f32)
+
+    bottom = pl.ds(total_rows, edge)
+    hg_v[bottom, :] = jnp.ones((edge, channels), f32)
+    a_v[bottom, :] = edge_recv[...]
+    b_v[bottom, :] = pltpu.roll(edge_recv[...], edge - 2, 0)
+    tap_mine[...] = jnp.zeros(tap_mine.shape, f32)
+    lax.fori_loop(0, lane_tiles, grad_last, 0)
+    store_gate = pltpu.make_async_copy(
+        gate_v.at[pl.ds(BF16_ROWS, total_rows)], gate_out, local.at[4]
+    )
+    store_up = pltpu.make_async_copy(up_v.at[pl.ds(BF16_ROWS, total_rows)], up_out, local.at[5])
+    store_gate.start()
+    store_up.start()
+
+    tap_pair_copy = remote(
+        tap_mine.at[1 - core], tap_pair, tp_send.at[0], tp_recv.at[0], {"fs": partner}
+    )
+    tap_pair_copy.start()
+
+    def tap_chip_copy(i, sender):
+        return remote(
+            tap_chip.at[sender],
+            tap_chip.at[sender],
+            tz_send.at[i],
+            tz_recv.at[sender],
+            {"fs": ((z + i) % chips) * 2 + core},
+        )
+
+    tap_pair_copy.wait_recv()
+    tap_chip[z] = tap_mine[core] + tap_pair[...]
+    for i in range(1, chips):
+        tap_chip_copy(i, z).start()
+    for i in range(1, chips):
+        tap_chip_copy(i, (z + i) % chips).wait_recv()
+    total = tap_chip[0]
+    for i in range(1, chips):
+        total = total + tap_chip[i]
+    tap_all[core, q] = total * scale
+
+    def tap_all_copy(i, sender):
+        return remote(
+            tap_all.at[core, sender],
+            tap_all.at[core, sender],
+            ta_send.at[i],
+            ta_recv.at[sender],
+            {"tp": (q + i) % tps},
+        )
+
+    for i in range(1, tps):
+        tap_all_copy(i, q).start()
+
+    for s in range(PIECES):
+        slot(chips - 1, s)
+
+    ones = jnp.ones((8, cols), bf16)
+
+    def finish(s, carry):
+        here = pl.ds(pl.multiple_of(s * piece, BF16_ROWS), piece)
+        value = dg_v[here, :]
+        value = value + jnp.where(z > 0, rs_recv[0, z, here, :].astype(f32), 0.0)
+        value = value + jnp.where(z < chips - 1, rs_recv[1, z, here, :].astype(f32), 0.0)
+        dg_v[here, :] = value * scale
+        return carry
+
+    lax.fori_loop(0, PIECES, finish, 0)
+    store_down = pltpu.make_async_copy(dg_v, down_out, local.at[6])
+    store_down.start()
+    contract = (((1,), (1,)), ((), ()))
+    value = dg_v[...]
+    square = value * value
+    high = square.astype(bf16)
+    low = (square - high.astype(f32)).astype(bf16)
+    norm = lax.dot_general(ones, high, contract, preferred_element_type=f32)
+    norm = norm + lax.dot_general(ones, low, contract, preferred_element_type=f32)
+    norm_all[f] = norm[0:1]
+
+    def norm_copy(i, sender):
+        return remote(
+            norm_all.at[sender],
+            norm_all.at[sender],
+            n_send.at[i],
+            n_recv.at[sender],
+            {"fs": (f + i) % fs},
+        )
+
+    for i in range(1, fs):
+        norm_copy(i, f).start()
+    for i in range(1, tps):
+        tap_all_copy(i, (q + i) % tps).wait_recv()
+
+    def tap_both_copy(which):
+        return remote(
+            tap_all.at[which], tap_all.at[which], tb_send.at[0], tb_recv.at[0], {"fs": partner}
+        )
+
+    tap_both_copy(core).start()
+    for i in range(1, fs):
+        norm_copy(i, (f + i) % fs).wait_recv()
+    total = norm_all[0]
+    for i in range(1, fs):
+        total = total + norm_all[i]
+    norm_out[...] = total * (1.0 / features)
+    tap_both_copy(1 - core).wait_recv()
+    for b in range(2):
+        for i in range(tps):
+            taps_out[b, :, i * channels : (i + 1) * channels] = tap_all[b, i, 0:3, :]
+
+    store_gate.wait()
+    store_up.wait()
+    store_down.wait()
+
+    @pl.when(f < fs - 1)
+    def _():
+        halo_copy(0, gate_ref, gate_v).wait_send()
+        halo_copy(1, up_ref, up_v).wait_send()
+
+    @pl.when(f > 0)
+    def _():
+        edge_copy.wait_send()
+
+    for k in range(chips):
+        for way in range(2):
+            for step in range(1, half_ring + 1):
+                ring_copy(k, step, way).wait_send()
+        pair_terms_copy(k).wait_send()
+        for s in range(PIECES):
+            pair_down(k, core, s).wait_send()
+
+    for p in range(chips):
+        for s in range(PIECES):
+            where = rs_send.at[0, pl.ds(s * piece, piece)]
+
+            @pl.when(z < chips - 1)
+            def _():
+                z_copy(where, where, 0, p, s).wait_send()
+
+            @pl.when(z > 0)
+            def _():
+                z_copy(where, where, 1, p, s).wait_send()
+
+    tap_pair_copy.wait_send()
+    tap_both_copy(core).wait_send()
+    for i in range(1, chips):
+        tap_chip_copy(i, z).wait_send()
+    for i in range(1, tps):
+        tap_all_copy(i, q).wait_send()
+    for i in range(1, fs):
+        norm_copy(i, f).wait_send()
+
+
+def whole_body(gate_pre, up_pre, gate_taps, up_taps, down_proj, cotangent):
+    fs, tps = lax.axis_size("fs"), lax.axis_size("tp")
+    chips = fs // 2
+    rows, features = cotangent.shape
+    channels, cols = down_proj.shape
+    total = rows * tps
+    f32, bf16 = jnp.float32, jnp.bfloat16
+    dma = pltpu.SemaphoreType.DMA
+    scale = 1.0 / math.sqrt(total * fs)
+    ring = (chips, 2, tps // 2)
+    gate_grad, up_grad, down_grad, norms, taps = pl.pallas_call(
+        functools.partial(whole_kernel, chips, tps, scale),
+        out_shape=(
+            jax.ShapeDtypeStruct((total, channels), bf16),
+            jax.ShapeDtypeStruct((total, channels), bf16),
+            jax.ShapeDtypeStruct((channels, cols), f32),
+            jax.ShapeDtypeStruct((1, channels), f32),
+            jax.ShapeDtypeStruct((2, 3, channels * tps), f32),
+        ),
+        in_specs=[
+            pl.BlockSpec(memory_space=pl.ANY),
+            pl.BlockSpec(memory_space=pl.ANY),
+            pl.BlockSpec(memory_space=pltpu.VMEM),
+            pl.BlockSpec(memory_space=pltpu.VMEM),
+            pl.BlockSpec(memory_space=pl.ANY),
+            pl.BlockSpec(memory_space=pl.ANY),
+        ],
+        out_specs=[
+            pl.BlockSpec(memory_space=pl.ANY),
+            pl.BlockSpec(memory_space=pl.ANY),
+            pl.BlockSpec(memory_space=pl.ANY),
+            pl.BlockSpec(memory_space=pltpu.VMEM),
+            pl.BlockSpec(memory_space=pltpu.VMEM),
+        ],
+        scratch_shapes=[
+            pltpu.VMEM((total + BF16_ROWS, channels), bf16),
+            pltpu.VMEM((total + BF16_ROWS, channels), bf16),
+            pltpu.VMEM((2, 4, channels), f32),
+            pltpu.VMEM((total + 8, channels), f32),
+            pltpu.VMEM((total + 8, channels), f32),
+            pltpu.VMEM((channels, total), bf16),
+            pltpu.VMEM((total, features), bf16),
+            pltpu.VMEM((channels, features), bf16),
+            pltpu.VMEM((chips, channels, cols), bf16),
+            pltpu.VMEM((chips, channels, cols), bf16),
+            pltpu.VMEM((2, chips, channels, cols), bf16),
+            pltpu.VMEM((chips, channels, cols), bf16),
+            pltpu.VMEM((channels, cols), f32),
+            pltpu.VMEM((total + 8, channels), f32),
+            pltpu.VMEM((8, channels), f32),
+            pltpu.VMEM((8, channels), f32),
+            pltpu.VMEM((6, 8, channels), f32),
+            pltpu.VMEM((2, 4, channels), f32),
+            pltpu.VMEM((4, channels), f32),
+            pltpu.VMEM((chips, 4, channels), f32),
+            pltpu.VMEM((2, tps, 4, channels), f32),
+            pltpu.VMEM((fs, 1, channels), f32),
+            dma((7,)),
+            dma((2, chips, PIECES)),
+            dma((2, chips, PIECES)),
+            dma((chips, PIECES)),
+            dma((chips, PIECES)),
+            dma((chips,)),
+            dma((chips,)),
+            dma(ring),
+            dma(ring),
+            dma((2,)),
+            dma((2,)),
+            dma((1,)),
+            dma((1,)),
+            dma((1,)),
+            dma((1,)),
+            dma((chips,)),
+            dma((chips,)),
+            dma((tps,)),
+            dma((tps,)),
+            dma((1,)),
+            dma((1,)),
+            dma((fs,)),
+            dma((fs,)),
+        ],
+        compiler_params=pltpu.CompilerParams(
+            collective_id=2, has_side_effects=True, vmem_limit_bytes=VMEM_BYTES
+        ),
+        name="whole_layer",
+    )(gate_pre, up_pre, gate_taps, up_taps, down_proj, cotangent)
+    return gate_grad, up_grad, down_grad, norms.reshape(channels), taps
+
+
+VMEM_BYTES = 67_043_328
+
+
+def fits_whole(gate_pre, gate_taps, down_proj, cotangent):
+    fs, tps = lax.axis_size("fs"), lax.axis_size("tp")
+    chips = fs // 2
+    channels, cols = down_proj.shape
+    rows, features = cotangent.shape
+    total = rows * tps
+    tiled = channels % (LANES * PIECES // 2) == 0 and cols % (2 * LANES) == 0
+    tiled = tiled and channels % (BF16_ROWS * PIECES) == 0 and total % ROW_TILE == 0
+    tiled = tiled and rows % (2 * BF16_ROWS) == 0 and gate_taps.shape[0] == 3
+    tiled = tiled and fs % 2 == 0 and chips % 2 == 0 and chips >= 4 and tps >= 4
+    held = 2 * total * channels * (2 + 4) + total * channels * (2 + 4)
+    held += (total + channels) * features * 2 + channels * cols * (5 * chips * 2 + 4)
+    return tiled and held < VMEM_BYTES * 7 // 8
+
+
+def body(gate_pre, up_pre, gate_taps, up_taps, down_proj, cotangent):
+    args = (gate_pre, up_pre, gate_taps, up_taps, down_proj, cotangent)
+    if fits_whole(gate_pre, gate_taps, down_proj, cotangent):
+        return whole_body(*args)
+    return staged_body(*args)
+
+
 def solution(mesh):
     placed = (P("fs", "tp"), P("fs", "tp"), P(), P(), P("tp", "fs"), P(("fs", "tp"), None))
     return jax.shard_map(

time: 197 us -> 95.5 us (0.48)
  other arithmetic: 55.3 us -> 1.31 us
  matrix products: 22.8 us -> 0 us
  waiting for transfers between devices: 16 us -> 0 us
  between operations: 14.3 us -> 0.65 us
  Pallas kernels: 72.1 us -> 84.3 us
  starting transfers between devices: 9.84 us -> 0 us
  local copies, waits for them, and re-layouts: 5.98 us -> 8.91 us
    convert_element_type x6 -> x0, other arithmetic: 36.4 us -> none  [the longest x1 12.8 us: body(): hidden = (gate_act * up_conv).astype(jnp.bfloat16)]
    dot_general x2 -> x0, matrix products: 22.8 us -> none  [the longest x1 11.9 us: body(): lax.dot_general(whole_cot, whole_down, (((1,), (1,)), ((), ())), preferre...]
    reduce_scatter x1 -> x0, waiting for transfers between devices: 16 us -> none  [body(): own_rows = lax.psum_scatter(terms, 'fs', scatter_dimension=0, tiled=True)]
    reduce_sum x2 -> x0, other arithmetic: 15.8 us -> none  [the longest x1 14.5 us: body(): jnp.sum(up_conv_grad * up_padded[offset:offset + row_count], axis=0)]
    pallas_call x2 -> x1, Pallas kernels: 72.1 us -> 84.3 us  [whole_body(): pl.pallas_call(functools.partial(whole_kernel, chips, tps, scale), out_sh...]
    ppermute x4 -> x0, starting transfers between devices: 9.8 us -> none  [from_behind(): return lax.ppermute(block, axis, route)]
    unnamed x16 -> x8, local copies, waits for them, and re-layouts: 2.4 us -> 8.91 us
    slice x6 -> x0, local copies, waits for them, and re-layouts: 3.33 us -> none  [the longest x1 0.94 us: body(): gate_conv_grad[0:reach]]
  transfers between devices with their start and end apart: 5 -> 0, of which waited for: 1 -> 0; matrix products, arithmetic and copies ran while one was open for 25% -> 0% of each run, Pallas kernels for 29% -> 0%
where the time goes in v1:
time: 95.5 us; the launch traced here: 95.2 us
  Pallas kernels  84.3 us (88%)
  local copies, waits for them, and re-layouts  8.91 us (9%)
  other arithmetic  1.31 us (1%)
    pallas_call x1, Pallas kernels, whole_body(): pl.pallas_call(functools.partial(whole_kernel, chips, tps, scale), out_sh...  84.3 us
    unnamed x8, local copies, waits for them, and re-layouts  8.91 us

profile of v1, /device:TPU:0, one launch (start us, length us, event | category | flops | bytes accessed | tf_op | source)
XLA Modules:
  0.0 95.2 jit_solution(14722050968539556016)
XLA Ops:
  0.6 84.3 %whole_layer.1 = (bf16[1024,1408]{1,0:T(8,128)(2,1)}, bf16[1024,1408]{1,0:T(8,128)(2,1)}, f32[1408,256]{1,0:T(8,128)}, f32[1,1408]{1,0:T(1,128)}, f32[2,3,5632]{2,1,0:T(4,128)}) custom-call(bf16[1024,1408]{1,0:T(8,128)(2,1)} %gate_ref.1, bf16[1024,1408]{1,0:T(8,128)(2,1)} %up_ref.1, bf16[3,5632]{1,0:T(4,128)(2,1)} %gtaps_ref.1, bf16[3,5632]{1,0:T(4,128)(2,1)} %utaps_ref.1, ...), custom_call_target="tpu_custom_call" | custom-call | tf_op jit(solution)/shard_map/whole_layer/pallas_call | solution.py:1052
  85.0 1.3 %reduce = f32[1408]{0:T(1024)} reduce(f32[1,1408]{1,0:T(1,128)} %get-tuple-element.13, f32[]{:T(128)} %constant), dimensions={0}, to_apply=%get-tuple-element.13.reduce_sub_computation | reduce | bytes 11268 | tf_op jit(solution)/shard_map/whole_layer/pallas_call | solution.py:1052
  86.3 1.6 %copy.11 = f32[2,3,5632]{2,0,1:T(2,128)} copy(f32[2,3,5632]{2,1,0:T(4,128)} %get-tuple-element.19) | data formatting | bytes 270336
  87.9 0.0 copy-start
  87.9 3.8 %copy.15 = bf16[1024,1408]{1,0:T(8,128)(2,1)} copy(bf16[1024,1408]{1,0:T(8,128)(2,1)} %get-tuple-element.25) | data formatting | bytes 5767168
  91.7 0.0 copy-done
  91.7 0.0 copy-start.1
  91.7 1.6 %copy.16 = bf16[1024,1408]{1,0:T(8,128)(2,1)} copy(bf16[1024,1408]{1,0:T(8,128)(2,1)S(1)} %copy-done) | data formatting | bytes 5767168
  93.3 0.8 copy-done.1
  94.1 1.1 %copy.17 = f32[1408,256]{1,0:T(8,128)} copy(f32[1408,256]{1,0:T(8,128)S(1)} %copy-done.1) | data formatting | bytes 2883584
Async XLA Ops:
  87.9 3.8 %copy-start = (bf16[1024,1408]{1,0:T(8,128)(2,1)S(1)}, bf16[1024,1408]{1,0:T(8,128)(2,1)}, u32[]{:S(2)}) copy-start(bf16[1024,1408]{1,0:T(8,128)(2,1)} %get-tuple-element.26) | copy-start | bytes 8650756
  91.7 2.4 %copy-start.1 = (f32[1408,256]{1,0:T(8,128)S(1)}, f32[1408,256]{1,0:T(8,128)}, u32[]{:S(2)}) copy-start(f32[1408,256]{1,0:T(8,128)} %get-tuple-element.27) | copy-start | bytes 4325380

commit v2 on v1

--- a/solution.py
+++ b/solution.py
@@ -394,12 +394,18 @@
     )
 
 
-PIECES = 2
+PIECES = 4
 ROW_TILE = 128
 SUB = 32
 BLOCK = 64
 LANES = 128
 BF16_ROWS = 16
+
+
+def cut(channels):
+    tiles = channels // LANES
+    sizes = [(tiles + PIECES - 1 - i) // PIECES * LANES for i in range(PIECES)]
+    return [(sum(sizes[:i]), sizes[i]) for i in range(PIECES)]
 
 
 def less(a, b):
@@ -423,6 +429,7 @@
     taps_out,
     gate_v,
     up_v,
+    tap_in,
     taps_v,
     a_v,
     b_v,
@@ -433,7 +440,7 @@
     pair_recv,
     rs_recv,
     rs_send,
-    dg_v,
+    own_v,
     hg_v,
     edge_send,
     edge_recv,
@@ -443,11 +450,12 @@
     tap_chip,
     tap_all,
     norm_all,
+    norm_v,
     *sems,
 ):
     (local, z_send, z_recv, pd_send, pd_recv, pt_send, pt_recv, c_send, c_recv) = sems[:9]
     (h_send, h_recv, e_send, e_recv, tp_send, tp_recv, tz_send, tz_recv) = sems[9:17]
-    (ta_send, ta_recv, tb_send, tb_recv, n_send, n_recv) = sems[17:]
+    (ta_send, ta_recv, n_send, n_recv, down_sem) = sems[17:]
     f, q = lax.axis_index("fs"), lax.axis_index("tp")
     z, core = f // 2, f % 2
     fs = 2 * chips
@@ -456,7 +464,7 @@
     channels, cols = down_ref.shape
     total_rows = rows * tps
     chip_cols = 2 * cols
-    piece = channels // PIECES
+    pieces = cut(channels)
     lane_tiles = channels // LANES
     half = z // (chips // 2)
     width = math.isqrt(tps)
@@ -477,7 +485,7 @@
 
     def down_piece(chip, which, s):
         col = pl.multiple_of(chip * chip_cols + which * cols, cols)
-        return down_v.at[pl.ds(s * piece, piece), pl.ds(col, cols)]
+        return down_v.at[pl.ds(*pieces[s]), pl.ds(col, cols)]
 
     own_cot = pltpu.make_async_copy(
         cot_ref, cot_v.at[pl.ds(pl.multiple_of(q * rows, rows), rows)], local.at[0]
@@ -491,8 +499,15 @@
         gate_ref, gate_v.at[pl.ds(BF16_ROWS, total_rows)], local.at[2]
     )
     load_up = pltpu.make_async_copy(up_ref, up_v.at[pl.ds(BF16_ROWS, total_rows)], local.at[3])
+    tap_col = pl.ds(pl.multiple_of(q * channels, LANES), channels)
+    load_taps = [
+        pltpu.make_async_copy(ref.at[:, tap_col], tap_in.at[b], local.at[7 + b])
+        for b, ref in enumerate((gtaps_ref, utaps_ref))
+    ]
     own_down.start()
     own_cot.start()
+    load_taps[0].start()
+    load_taps[1].start()
     load_gate.start()
     load_up.start()
 
@@ -501,7 +516,14 @@
         pl.semaphore_signal(barrier, inc=1, device_id={"fs": (f + i) % fs}, device_id_type=MESH)
     for i in range(1, tps):
         pl.semaphore_signal(barrier, inc=1, device_id={"tp": (q + i) % tps}, device_id_type=MESH)
-    pl.semaphore_wait(barrier, fs + tps - 2)
+    for i in range(1, tps):
+        pl.semaphore_signal(
+            barrier,
+            inc=1,
+            device_id={"fs": partner, "tp": (q + i) % tps},
+            device_id_type=MESH,
+        )
+    pl.semaphore_wait(barrier, fs + 2 * tps - 3)
 
     def chip_at(position, way):
         return position + way * (chips - 1 - 2 * position)
@@ -603,9 +625,9 @@
     for s in range(PIECES):
         pair_down(z, core, s).start()
 
-    tap_col = pl.multiple_of(q * channels, LANES)
-    taps_v[0, 0:3, :] = gtaps_ref[:, pl.ds(tap_col, channels)].astype(f32)
-    taps_v[1, 0:3, :] = utaps_ref[:, pl.ds(tap_col, channels)].astype(f32)
+    for b in range(2):
+        load_taps[b].wait()
+        taps_v[b, 0:3, :] = tap_in[b].astype(f32)
 
     def hidden_tile(tile, lane_tile):
         lane = pl.ds(pl.multiple_of(lane_tile * LANES, LANES), LANES)
@@ -636,19 +658,22 @@
         tile_t = jnp.concatenate(parts, axis=0).T
         hid_t[lane, pl.ds(pl.multiple_of(tile * ROW_TILE, ROW_TILE), ROW_TILE)] = tile_t
 
-    def hidden_tiles(first, count):
+    tiles = total_rows // ROW_TILE
+
+    def hidden_piece(s, first, count):
+        start, size = pieces[s]
+        lane_count = size // LANES
+
         def step(i, carry):
-            hidden_tile(first + i // lane_tiles, i % lane_tiles)
+            hidden_tile(first + i // lane_count, start // LANES + i % lane_count)
             return carry
 
-        lax.fori_loop(0, count * lane_tiles, step, 0)
-
-    tiles = total_rows // ROW_TILE
+        lax.fori_loop(0, count * lane_count, step, 0)
+
     load_gate.wait()
     load_up.wait()
-    hidden_tiles(tiles // 2, tiles - tiles // 2)
-    ring_step(0, 1)
-    hidden_tiles(1, tiles // 2 - 1)
+    hidden_piece(0, 1, tiles - 1)
+    hidden_piece(1, 1, tiles - 1)
 
     @pl.when(f > 0)
     def _():
@@ -660,46 +685,46 @@
         gate_v[0:BF16_ROWS, :] = jnp.zeros((BF16_ROWS, channels), bf16)
         up_v[0:BF16_ROWS, :] = jnp.zeros((BF16_ROWS, channels), bf16)
 
-    hidden_tiles(0, 1)
-
-    def terms(s, chip, which):
-        col = pl.multiple_of(chip * chip_cols + which * cols, cols)
-        return jnp.dot(
-            hid_t[pl.ds(pl.multiple_of(s * piece, BF16_ROWS), piece), :],
-            cot_v[:, pl.ds(col, cols)],
-            preferred_element_type=f32,
-        )
-
-    def pair_terms_copy(chip):
+    hidden_piece(0, 0, 1)
+    hidden_piece(1, 0, 1)
+    ring_step(0, 1)
+    hidden_piece(2, 0, tiles)
+    hidden_piece(3, 0, tiles)
+
+    def pair_terms_copy(chip, s):
+        here = pl.ds(*pieces[s])
         return remote(
-            pair_send.at[chip],
-            pair_recv.at[chip],
-            pt_send.at[chip],
-            pt_recv.at[chip],
+            pair_send.at[chip, here],
+            pair_recv.at[chip, here],
+            pt_send.at[chip, s],
+            pt_recv.at[chip, s],
             {"fs": partner},
         )
 
     def pair_terms(k):
         chip = chunk_chip(k)
-
-        def step(s, carry):
-            here = pl.ds(pl.multiple_of(s * piece, BF16_ROWS), piece)
-            pair_send[chip, here, :] = terms(s, chip, 1 - core).astype(bf16)
-            return carry
-
-        lax.fori_loop(0, PIECES, step, 0)
-        pair_terms_copy(chip).start()
-
-    def pair_terms_wait(k):
-        pair_terms_copy(chunk_chip(k)).wait_recv()
+        both = cot_v[:, pl.ds(pl.multiple_of(chip * chip_cols, chip_cols), chip_cols)]
+        mid = PIECES // 2
+        for group in (range(mid), range(mid, PIECES)):
+            start = pieces[group[0]][0]
+            size = sum(pieces[s][1] for s in group)
+            here = pl.ds(start, size)
+            value = jnp.dot(hid_t[here, :], both, preferred_element_type=f32)
+            low, high = value[:, :cols], value[:, cols:]
+            pair_send[chip, here, :] = jnp.where(core == 0, high, low).astype(bf16)
+            for s in group:
+                pair_terms_copy(chip, s).start()
+            own_v[chip, here, :] = jnp.where(core == 0, low, high)
+
+    def pair_terms_wait(k, s):
+        pair_terms_copy(chunk_chip(k), s).wait_recv()
 
     def send_sum(position, way, p, s, first):
         chip = chip_at(chips - 1 + position - p, way)
-        here = pl.ds(s * piece, piece)
-        value = terms(s, chip, core) + pair_recv[chip, here, :].astype(f32)
+        here = pl.ds(*pieces[s])
+        value = own_v[chip, here, :] + pair_recv[chip, here, :].astype(f32)
         if not first:
-            earlier = rs_recv[way, chip, here, :].astype(f32)
-            value = value + jnp.where(position > 0, earlier, 0.0)
+            value = value + rs_recv[way, chip, here, :].astype(f32)
         rs_send[chip, here, :] = value.astype(bf16)
         z_copy(rs_send.at[chip, here], rs_recv.at[way, chip, here], way, p + 1, s).start()
 
@@ -711,43 +736,45 @@
 
         lax.fori_loop(0, 2, step, 0)
 
-    def first_sums():
+    def first_sum(p, s):
         def body(way, position):
             @pl.when(position == 0)
             def _():
-                for s in range(PIECES):
-                    send_sum(position, way, 0, s, True)
+                send_sum(position, way, p, s, True)
 
         both_ways(body)
 
-    def slot(p, s):
-        here = pl.ds(s * piece, piece)
+    def slot(p, s, arrive=True, send=True):
+        here = pl.ds(*pieces[s])
 
         def body(way, position):
-            @pl.when(position > p)
-            def _():
-                chip = chip_at(position - 1 - p, way)
-                where = down_piece(chip, core, s)
-                z_copy(where, where, way, p, s).wait_recv()
-                if p + 1 < chips:
-
-                    @pl.when(position < chips - 1)
+            if arrive:
+
+                @pl.when(position > p)
+                def _():
+                    chip = chip_at(position - 1 - p, way)
+                    where = down_piece(chip, core, s)
+                    z_copy(where, where, way, p, s).wait_recv()
+                    if p + 1 < chips:
+
+                        @pl.when(position < chips - 1)
+                        def _():
+                            z_copy(where, where, way, p + 1, s).start()
+
+                    pair_down(chip, core, s).start()
+
+            if p > 0:
+                if arrive:
+
+                    @pl.when(jnp.logical_and(position > 0, position <= p))
                     def _():
-                        z_copy(where, where, way, p + 1, s).start()
-
-                pair_down(chip, core, s).start()
-
-            if p > 0:
-
-                @pl.when(jnp.logical_and(position > 0, position <= p))
-                def _():
-                    chip = chip_at(chips - 1 + position - p, way)
-                    where = rs_recv.at[way, chip, here]
-                    z_copy(where, where, way, p, s).wait_recv()
-
-                if p + 1 < chips:
-
-                    @pl.when(position <= p)
+                        chip = chip_at(chips - 1 + position - p, way)
+                        where = rs_recv.at[way, chip, here]
+                        z_copy(where, where, way, p, s).wait_recv()
+
+                if send and p + 1 < chips:
+
+                    @pl.when(jnp.logical_and(position > 0, position <= p))
                     def _():
                         send_sum(position, way, p, s, False)
 
@@ -785,41 +812,55 @@
         if channels % wide:
             one(channels - channels % wide, channels % wide)
 
-    slot(0, 0)
-    for step in range(2, half_ring + 1):
-        ring_step(0, step)
-    pair_terms(0)
-    pair_terms_wait(0)
-    first_sums()
-    for s in range(1, PIECES):
+    def ring_ends(k):
+        for step in range(2, half_ring + 1):
+            ring_step(k, step)
+
+    def ready(k):
+        ring_ends(k)
+        pair_terms(k)
+
+    def start_sums(k):
+        for s in range(PIECES):
+            pair_terms_wait(k, s)
+            first_sum(k, s)
+
+    mid = PIECES // 2
+    for s in range(mid):
+        slot(0, s)
+    ready(0)
+    start_sums(0)
+    for s in range(mid, PIECES):
         slot(0, s)
     ring_step(1, 1)
-    for p in range(1, chips - 1):
+    for p in range(1, chips - 2):
+        slot(p, 0)
         ring_step(p + 1, 1)
-        for step in range(2, half_ring + 1):
-            ring_step(p, step)
+        ring_ends(p)
+        for s in range(1, mid):
+            slot(p, s)
         pair_terms(p)
-        pair_terms_wait(p)
-        if p < chips - 2:
-            for s in range(PIECES):
-                slot(p, s)
-    for step in range(2, half_ring + 1):
-        ring_step(chips - 1, step)
-    pair_terms(chips - 1)
+        start_sums(p)
+        for s in range(mid, PIECES):
+            slot(p, s)
+    ring_step(chips - 1, 1)
+    ready(chips - 2)
+    for s in range(mid):
+        pair_terms_wait(chips - 2, s)
     slot(chips - 2, 0)
+    first_sum(chips - 2, 0)
+    ready(chips - 1)
     for i in range(chips - 1):
         pair_down_wait(half + i)
     hidden_grad(half, chips - 1, False)
-    pair_terms_wait(chips - 1)
-    for s in range(1, PIECES):
+    for s in range(1, mid):
+        first_sum(chips - 2, s)
+    for s in range(PIECES):
+        pair_terms_wait(chips - 1, s)
+    for s in range(1, mid):
         slot(chips - 2, s)
-
-    def own_terms(s, carry):
-        here = pl.ds(pl.multiple_of(s * piece, BF16_ROWS), piece)
-        dg_v[here, :] = terms(s, z, core) + pair_recv[z, here, :].astype(f32)
-        return carry
-
-    lax.fori_loop(0, PIECES, own_terms, 0)
+    for s in range(mid, PIECES):
+        slot(chips - 2, s, send=False)
     pair_down_wait(last_chip)
     hidden_grad(last_chip, 1, True)
 
@@ -838,6 +879,11 @@
     @pl.when(f > 0)
     def _():
         edge_copy.start()
+
+    for s in range(mid, PIECES):
+        pair_terms_wait(chips - 2, s)
+        first_sum(chips - 2, s)
+        slot(chips - 2, s, arrive=False)
 
     def grads(start, lane, sums):
         window = pl.ds(start, BLOCK + edge)
@@ -903,6 +949,10 @@
     store_gate.start()
     store_up.start()
 
+    def store_down(s):
+        here = pl.ds(*pieces[s])
+        return pltpu.make_async_copy(own_v.at[z, here], down_out.at[here], down_sem.at[s])
+
     tap_pair_copy = remote(
         tap_mine.at[1 - core], tap_pair, tp_send.at[0], tp_recv.at[0], {"fs": partner}
     )
@@ -921,49 +971,24 @@
     tap_chip[z] = tap_mine[core] + tap_pair[...]
     for i in range(1, chips):
         tap_chip_copy(i, z).start()
-    for i in range(1, chips):
-        tap_chip_copy(i, (z + i) % chips).wait_recv()
-    total = tap_chip[0]
-    for i in range(1, chips):
-        total = total + tap_chip[i]
-    tap_all[core, q] = total * scale
-
-    def tap_all_copy(i, sender):
-        return remote(
-            tap_all.at[core, sender],
-            tap_all.at[core, sender],
-            ta_send.at[i],
-            ta_recv.at[sender],
-            {"tp": (q + i) % tps},
-        )
-
-    for i in range(1, tps):
-        tap_all_copy(i, q).start()
-
+
+    ones = jnp.ones((8, cols), bf16)
+    contract = (((1,), (1,)), ((), ()))
     for s in range(PIECES):
         slot(chips - 1, s)
-
-    ones = jnp.ones((8, cols), bf16)
-
-    def finish(s, carry):
-        here = pl.ds(pl.multiple_of(s * piece, BF16_ROWS), piece)
-        value = dg_v[here, :]
+        here = pl.ds(*pieces[s])
+        value = own_v[z, here, :] + pair_recv[z, here, :].astype(f32)
         value = value + jnp.where(z > 0, rs_recv[0, z, here, :].astype(f32), 0.0)
         value = value + jnp.where(z < chips - 1, rs_recv[1, z, here, :].astype(f32), 0.0)
-        dg_v[here, :] = value * scale
-        return carry
-
-    lax.fori_loop(0, PIECES, finish, 0)
-    store_down = pltpu.make_async_copy(dg_v, down_out, local.at[6])
-    store_down.start()
-    contract = (((1,), (1,)), ((), ()))
-    value = dg_v[...]
-    square = value * value
-    high = square.astype(bf16)
-    low = (square - high.astype(f32)).astype(bf16)
-    norm = lax.dot_general(ones, high, contract, preferred_element_type=f32)
-    norm = norm + lax.dot_general(ones, low, contract, preferred_element_type=f32)
-    norm_all[f] = norm[0:1]
+        value = value * scale
+        own_v[z, here, :] = value
+        store_down(s).start()
+        square = value * value
+        high = square.astype(bf16)
+        low = (square - high.astype(f32)).astype(bf16)
+        norm = lax.dot_general(ones, high, contract, preferred_element_type=f32)
+        norm = norm + lax.dot_general(ones, low, contract, preferred_element_type=f32)
+        norm_all[f, :, here] = norm[0:1]
 
     def norm_copy(i, sender):
         return remote(
@@ -976,67 +1001,142 @@
 
     for i in range(1, fs):
         norm_copy(i, f).start()
-    for i in range(1, tps):
-        tap_all_copy(i, (q + i) % tps).wait_recv()
-
-    def tap_both_copy(which):
+    @pl.when(f < fs - 1)
+    def _():
+        halo_copy(0, gate_ref, gate_v).wait_send()
+        halo_copy(1, up_ref, up_v).wait_send()
+
+    @pl.when(f > 0)
+    def _():
+        edge_copy.wait_send()
+
+    for k in range(chips):
+        for way in range(2):
+            for step in range(1, half_ring + 1):
+                ring_copy(k, step, way).wait_send()
+        for s in range(PIECES):
+            pair_terms_copy(k, s).wait_send()
+        for s in range(PIECES):
+            pair_down(k, core, s).wait_send()
+
+    for p in range(chips):
+        for s in range(PIECES):
+            where = rs_send.at[0, pl.ds(*pieces[s])]
+
+            @pl.when(z < chips - 1)
+            def _():
+                z_copy(where, where, 0, p, s).wait_send()
+
+            @pl.when(z > 0)
+            def _():
+                z_copy(where, where, 1, p, s).wait_send()
+
+    for i in range(1, chips):
+        tap_chip_copy(i, (z + i) % chips).wait_recv()
+    total = tap_chip[0]
+    for i in range(1, chips):
+        total = total + tap_chip[i]
+    tap_all[core, q] = total * scale
+
+    def tap_all_copy(j, i, which, sender):
+        to = core if j == 0 else 1 - core
         return remote(
-            tap_all.at[which], tap_all.at[which], tb_send.at[0], tb_recv.at[0], {"fs": partner}
-        )
-
-    tap_both_copy(core).start()
+            tap_all.at[which, sender],
+            tap_all.at[which, sender],
+            ta_send.at[j, i],
+            ta_recv.at[which, sender],
+            {"fs": z * 2 + to, "tp": (q + i) % tps},
+        )
+
+    others = [(j, i) for i in range(tps) for j in range(2) if (j, i) != (0, 0)]
+    for j, i in others:
+        tap_all_copy(j, i, core, q).start()
     for i in range(1, fs):
         norm_copy(i, (f + i) % fs).wait_recv()
     total = norm_all[0]
     for i in range(1, fs):
         total = total + norm_all[i]
-    norm_out[...] = total * (1.0 / features)
-    tap_both_copy(1 - core).wait_recv()
-    for b in range(2):
-        for i in range(tps):
-            taps_out[b, :, i * channels : (i + 1) * channels] = tap_all[b, i, 0:3, :]
-
+    norm_v[...] = total * (1.0 / features)
+    store_norm = pltpu.make_async_copy(norm_v, norm_out, local.at[9])
+    store_norm.start()
+    for j, i in others:
+        which = core if j == 0 else 1 - core
+        tap_all_copy(j, i, which, (q + i) % tps).wait_recv()
+    store_taps = pltpu.make_async_copy(tap_all, taps_out, local.at[10])
+    store_taps.start()
+
+    store_norm.wait()
+    store_taps.wait()
     store_gate.wait()
     store_up.wait()
-    store_down.wait()
-
-    @pl.when(f < fs - 1)
-    def _():
-        halo_copy(0, gate_ref, gate_v).wait_send()
-        halo_copy(1, up_ref, up_v).wait_send()
-
-    @pl.when(f > 0)
-    def _():
-        edge_copy.wait_send()
-
-    for k in range(chips):
-        for way in range(2):
-            for step in range(1, half_ring + 1):
-                ring_copy(k, step, way).wait_send()
-        pair_terms_copy(k).wait_send()
-        for s in range(PIECES):
-            pair_down(k, core, s).wait_send()
-
-    for p in range(chips):
-        for s in range(PIECES):
-            where = rs_send.at[0, pl.ds(s * piece, piece)]
-
-            @pl.when(z < chips - 1)
-            def _():
-                z_copy(where, where, 0, p, s).wait_send()
-
-            @pl.when(z > 0)
-            def _():
-                z_copy(where, where, 1, p, s).wait_send()
+    for s in range(PIECES):
+        store_down(s).wait()
 
     tap_pair_copy.wait_send()
-    tap_both_copy(core).wait_send()
     for i in range(1, chips):
         tap_chip_copy(i, z).wait_send()
-    for i in range(1, tps):
-        tap_all_copy(i, q).wait_send()
+    for j, i in others:
+        tap_all_copy(j, i, core, q).wait_send()
     for i in range(1, fs):
         norm_copy(i, f).wait_send()
+
+
+def hand_over_kernel(*refs):
+    gate_ref, up_ref, down_ref, norm_ref, taps_ref = refs[:5]
+    gate_out, up_out, down_out, norm_out, taps_out = refs[5:10]
+    gate_v, up_v, down_v, sem_in, sem_out = refs[10:]
+    moves = []
+    for src, mid, dst in (
+        (gate_ref, gate_v, gate_out),
+        (up_ref, up_v, up_out),
+        (down_ref, down_v, down_out),
+    ):
+        rows = src.shape[0]
+        parts = 4 if src.shape[0] % 64 == 0 else 1
+        for i in range(parts):
+            here = pl.ds(i * (rows // parts), rows // parts)
+            moves.append((src.at[here], mid.at[here], dst.at[here]))
+    first = [
+        pltpu.make_async_copy(src, mid, sem_in.at[i]) for i, (src, mid, _) in enumerate(moves)
+    ]
+    second = [
+        pltpu.make_async_copy(mid, dst, sem_out.at[i]) for i, (_, mid, dst) in enumerate(moves)
+    ]
+    for copy in first:
+        copy.start()
+    channels = norm_ref.shape[1]
+    norm_out[...] = norm_ref[...]
+    for b in range(2):
+        for k in range(3):
+            for i in range(taps_ref.shape[1]):
+                taps_out[k, b : b + 1, i * channels : (i + 1) * channels] = taps_ref[
+                    b, i, k : k + 1, :
+                ]
+    for copy, after in zip(first, second):
+        copy.wait()
+        after.start()
+    for copy in second:
+        copy.wait()
+
+
+def hand_over(gate_grad, up_grad, down_grad, norms, taps):
+    tps, channels = taps.shape[1], taps.shape[3]
+    dma = pltpu.SemaphoreType.DMA
+    big = (gate_grad, up_grad, down_grad)
+    return pl.pallas_call(
+        hand_over_kernel,
+        out_shape=tuple(jax.ShapeDtypeStruct(a.shape, a.dtype) for a in big)
+        + (
+            jax.ShapeDtypeStruct((1, channels), jnp.float32),
+            jax.ShapeDtypeStruct((3, 2, channels * tps), jnp.float32),
+        ),
+        in_specs=[pl.BlockSpec(memory_space=pl.ANY)] * 3
+        + [pl.BlockSpec(memory_space=pltpu.VMEM)] * 2,
+        out_specs=[pl.BlockSpec(memory_space=pl.ANY)] * 3
+        + [pl.BlockSpec(memory_space=pltpu.VMEM)] * 2,
+        scratch_shapes=[pltpu.VMEM(a.shape, a.dtype) for a in big] + [dma((12,)), dma((12,))],
+        name="hand_over",
+    )(*big, norms, taps)
 
 
 def whole_body(gate_pre, up_pre, gate_taps, up_taps, down_proj, cotangent):
@@ -1056,26 +1156,17 @@
             jax.ShapeDtypeStruct((total, channels), bf16),
             jax.ShapeDtypeStruct((channels, cols), f32),
             jax.ShapeDtypeStruct((1, channels), f32),
-            jax.ShapeDtypeStruct((2, 3, channels * tps), f32),
+            jax.ShapeDtypeStruct((2, tps, 4, channels), f32),
         ),
         in_specs=[
-            pl.BlockSpec(memory_space=pl.ANY),
-            pl.BlockSpec(memory_space=pl.ANY),
-            pl.BlockSpec(memory_space=pltpu.VMEM),
-            pl.BlockSpec(memory_space=pltpu.VMEM),
-            pl.BlockSpec(memory_space=pl.ANY),
-            pl.BlockSpec(memory_space=pl.ANY),
-        ],
-        out_specs=[
-            pl.BlockSpec(memory_space=pl.ANY),
-            pl.BlockSpec(memory_space=pl.ANY),
-            pl.BlockSpec(memory_space=pl.ANY),
-            pl.BlockSpec(memory_space=pltpu.VMEM),
-            pl.BlockSpec(memory_space=pltpu.VMEM),
-        ],
+            pl.BlockSpec(memory_space=pl.ANY)
+        ]
+        * 6,
+        out_specs=[pl.BlockSpec(memory_space=pl.ANY)] * 5,
         scratch_shapes=[
             pltpu.VMEM((total + BF16_ROWS, channels), bf16),
             pltpu.VMEM((total + BF16_ROWS, channels), bf16),
+            pltpu.VMEM((2, 3, channels), bf16),
             pltpu.VMEM((2, 4, channels), f32),
             pltpu.VMEM((total + 8, channels), f32),
             pltpu.VMEM((total + 8, channels), f32),
@@ -1086,7 +1177,7 @@
             pltpu.VMEM((chips, channels, cols), bf16),
             pltpu.VMEM((2, chips, channels, cols), bf16),
             pltpu.VMEM((chips, channels, cols), bf16),
-            pltpu.VMEM((channels, cols), f32),
+            pltpu.VMEM((chips, channels, cols), f32),
             pltpu.VMEM((total + 8, channels), f32),
             pltpu.VMEM((8, channels), f32),
             pltpu.VMEM((8, channels), f32),
@@ -1096,13 +1187,14 @@
             pltpu.VMEM((chips, 4, channels), f32),
             pltpu.VMEM((2, tps, 4, channels), f32),
             pltpu.VMEM((fs, 1, channels), f32),
-            dma((7,)),
+            pltpu.VMEM((1, channels), f32),
+            dma((11,)),
             dma((2, chips, PIECES)),
             dma((2, chips, PIECES)),
             dma((chips, PIECES)),
             dma((chips, PIECES)),
-            dma((chips,)),
-            dma((chips,)),
+            dma((chips, PIECES)),
+            dma((chips, PIECES)),
             dma(ring),
             dma(ring),
             dma((2,)),
@@ -1113,22 +1205,25 @@
             dma((1,)),
             dma((chips,)),
             dma((chips,)),
-            dma((tps,)),
-            dma((tps,)),
-            dma((1,)),
-            dma((1,)),
+            dma((2, tps)),
+            dma((2, tps)),
             dma((fs,)),
             dma((fs,)),
+            dma((PIECES,)),
         ],
         compiler_params=pltpu.CompilerParams(
             collective_id=2, has_side_effects=True, vmem_limit_bytes=VMEM_BYTES
         ),
         name="whole_layer",
     )(gate_pre, up_pre, gate_taps, up_taps, down_proj, cotangent)
-    return gate_grad, up_grad, down_grad, norms.reshape(channels), taps
-
-
-VMEM_BYTES = 67_043_328
+    gate_grad, up_grad, down_grad, norms, taps = hand_over(
+        gate_grad, up_grad, down_grad, norms, taps
+    )
+    return gate_grad, up_grad, down_grad, norms.reshape(channels), taps.transpose(1, 0, 2)
+
+
+VMEM_BYTES = 64_000_000
+SPARE_BYTES = 5_000_000
 
 
 def fits_whole(gate_pre, gate_taps, down_proj, cotangent):
@@ -1137,13 +1232,13 @@
     channels, cols = down_proj.shape
     rows, features = cotangent.shape
     total = rows * tps
-    tiled = channels % (LANES * PIECES // 2) == 0 and cols % (2 * LANES) == 0
-    tiled = tiled and channels % (BF16_ROWS * PIECES) == 0 and total % ROW_TILE == 0
+    tiled = channels % LANES == 0 and cols % (2 * LANES) == 0
+    tiled = tiled and channels >= LANES * PIECES and total % ROW_TILE == 0
     tiled = tiled and rows % (2 * BF16_ROWS) == 0 and gate_taps.shape[0] == 3
     tiled = tiled and fs % 2 == 0 and chips % 2 == 0 and chips >= 4 and tps >= 4
     held = 2 * total * channels * (2 + 4) + total * channels * (2 + 4)
-    held += (total + channels) * features * 2 + channels * cols * (5 * chips * 2 + 4)
-    return tiled and held < VMEM_BYTES * 7 // 8
+    held += (total + channels) * features * 2 + channels * cols * chips * (5 * 2 + 4)
+    return tiled and held + SPARE_BYTES < VMEM_BYTES
 
 
 def body(gate_pre, up_pre, gate_taps, up_taps, down_proj, cotangent):

time: 95.5 us -> 88.3 us (0.925)
  local copies, waits for them, and re-layouts: 8.91 us -> 0 us
  Pallas kernels: 84.3 us -> 86.1 us
    unnamed x8 -> x0, local copies, waits for them, and re-layouts: 8.91 us -> none
    pallas_call x0 -> x1, Pallas kernels: none -> 7.37 us  [hand_over(): pl.pallas_call(hand_over_kernel, out_shape=tuple((jax.ShapeDtypeStruct(a....]
    pallas_call x1, Pallas kernels: 84.3 us -> 78.7 us  [whole_body(): pl.pallas_call(functools.partial(whole_kernel, chips, tps, scale), out_sh...]
where the time goes in v2:
time: 88.3 us; the launch traced here: 88.1 us
  Pallas kernels  86.1 us (98%)
  other arithmetic  1.31 us (1%)
    pallas_call x1, Pallas kernels, whole_body(): pl.pallas_call(functools.partial(whole_kernel, chips, tps, scale), out_sh...  78.7 us
    pallas_call x1, Pallas kernels, hand_over(): pl.pallas_call(hand_over_kernel, out_shape=tuple((jax.ShapeDtypeStruct(a....  7.37 us

profile of v2, /device:TPU:0, one launch (start us, length us, event | category | flops | bytes accessed | tf_op | source)
XLA Modules:
  0.0 88.1 jit_solution(12042165344730464247)
XLA Ops:
  0.6 78.7 %whole_layer.1 = (bf16[1024,1408]{1,0:T(8,128)(2,1)}, bf16[1024,1408]{1,0:T(8,128)(2,1)}, f32[1408,256]{1,0:T(8,128)}, f32[1,1408]{1,0:T(1,128)}, f32[2,4,4,1408]{3,2,1,0:T(4,128)}) custom-call(bf16[1024,1408]{1,0:T(8,128)(2,1)} %gate_ref.1, bf16[1024,1408]{1,0:T(8,128)(2,1)} %up_ref.1, bf16[3,5632]{1,0:T(4,128)(2,1)} %gtaps_ref.1, ...), custom_call_target="tpu_custom_call" | custom-call | tf_op jit(solution)/shard_map/whole_layer/pallas_call | solution.py:1152
  79.4 7.4 %hand_over.1 = (bf16[1024,1408]{1,0:T(8,128)(2,1)}, bf16[1024,1408]{1,0:T(8,128)(2,1)}, f32[1408,256]{1,0:T(8,128)}, f32[1,1408]{1,0:T(1,128)}, f32[3,2,5632]{2,1,0:T(2,128)}) custom-call(bf16[1024,1408]{1,0:T(8,128)(2,1)} %get-tuple-element.15.refs_0_, bf16[1024,1408]{1,0:T(8,128)(2,1)} %get-tuple-element.16.refs_1_, ...), custom_call_target="tpu_custom_call" | custom-call | tf_op jit(solution)/shard_map/hand_over/pallas_call | solution.py:1126
  86.8 1.3 %reduce = f32[1408]{0:T(1024)} reduce(f32[1,1408]{1,0:T(1,128)} %get-tuple-element.23, f32[]{:T(128)} %constant), dimensions={0}, to_apply=%get-tuple-element.23.reduce_sub_computation | reduce | bytes 11268 | tf_op jit(solution)/shard_map/hand_over/pallas_call | solution.py:1126

commit v3 on v2

--- a/solution.py
+++ b/solution.py
@@ -422,13 +422,11 @@
     utaps_ref,
     down_ref,
     cot_ref,
-    gate_out,
-    up_out,
-    down_out,
-    norm_out,
-    taps_out,
     gate_v,
     up_v,
+    down_out,
+    norm_v,
+    tap_all,
     tap_in,
     taps_v,
     a_v,
@@ -448,14 +446,12 @@
     tap_mine,
     tap_pair,
     tap_chip,
-    tap_all,
     norm_all,
-    norm_v,
     *sems,
 ):
     (local, z_send, z_recv, pd_send, pd_recv, pt_send, pt_recv, c_send, c_recv) = sems[:9]
     (h_send, h_recv, e_send, e_recv, tp_send, tp_recv, tz_send, tz_recv) = sems[9:17]
-    (ta_send, ta_recv, n_send, n_recv, down_sem) = sems[17:]
+    (ta_send, ta_recv, n_send, n_recv) = sems[17:]
     f, q = lax.axis_index("fs"), lax.axis_index("tp")
     z, core = f // 2, f % 2
     fs = 2 * chips
@@ -942,17 +938,6 @@
     b_v[bottom, :] = pltpu.roll(edge_recv[...], edge - 2, 0)
     tap_mine[...] = jnp.zeros(tap_mine.shape, f32)
     lax.fori_loop(0, lane_tiles, grad_last, 0)
-    store_gate = pltpu.make_async_copy(
-        gate_v.at[pl.ds(BF16_ROWS, total_rows)], gate_out, local.at[4]
-    )
-    store_up = pltpu.make_async_copy(up_v.at[pl.ds(BF16_ROWS, total_rows)], up_out, local.at[5])
-    store_gate.start()
-    store_up.start()
-
-    def store_down(s):
-        here = pl.ds(*pieces[s])
-        return pltpu.make_async_copy(own_v.at[z, here], down_out.at[here], down_sem.at[s])
-
     tap_pair_copy = remote(
         tap_mine.at[1 - core], tap_pair, tp_send.at[0], tp_recv.at[0], {"fs": partner}
     )
@@ -981,8 +966,7 @@
         value = value + jnp.where(z > 0, rs_recv[0, z, here, :].astype(f32), 0.0)
         value = value + jnp.where(z < chips - 1, rs_recv[1, z, here, :].astype(f32), 0.0)
         value = value * scale
-        own_v[z, here, :] = value
-        store_down(s).start()
+        down_out[here, :] = value
         square = value * value
         high = square.astype(bf16)
         low = (square - high.astype(f32)).astype(bf16)
@@ -1057,20 +1041,9 @@
     for i in range(1, fs):
         total = total + norm_all[i]
     norm_v[...] = total * (1.0 / features)
-    store_norm = pltpu.make_async_copy(norm_v, norm_out, local.at[9])
-    store_norm.start()
     for j, i in others:
         which = core if j == 0 else 1 - core
         tap_all_copy(j, i, which, (q + i) % tps).wait_recv()
-    store_taps = pltpu.make_async_copy(tap_all, taps_out, local.at[10])
-    store_taps.start()
-
-    store_norm.wait()
-    store_taps.wait()
-    store_gate.wait()
-    store_up.wait()
-    for s in range(PIECES):
-        store_down(s).wait()
 
     tap_pair_copy.wait_send()
     for i in range(1, chips):
@@ -1083,60 +1056,48 @@
 
 def hand_over_kernel(*refs):
     gate_ref, up_ref, down_ref, norm_ref, taps_ref = refs[:5]
-    gate_out, up_out, down_out, norm_out, taps_out = refs[5:10]
-    gate_v, up_v, down_v, sem_in, sem_out = refs[10:]
-    moves = []
-    for src, mid, dst in (
-        (gate_ref, gate_v, gate_out),
-        (up_ref, up_v, up_out),
-        (down_ref, down_v, down_out),
-    ):
-        rows = src.shape[0]
-        parts = 4 if src.shape[0] % 64 == 0 else 1
-        for i in range(parts):
-            here = pl.ds(i * (rows // parts), rows // parts)
-            moves.append((src.at[here], mid.at[here], dst.at[here]))
-    first = [
-        pltpu.make_async_copy(src, mid, sem_in.at[i]) for i, (src, mid, _) in enumerate(moves)
+    gate_out, up_out, down_out, norm_out, taps_out, sems = refs[5:]
+    rows = gate_out.shape[0]
+    copies = [
+        pltpu.make_async_copy(gate_ref.at[pl.ds(BF16_ROWS, rows)], gate_out, sems.at[0]),
+        pltpu.make_async_copy(up_ref.at[pl.ds(BF16_ROWS, rows)], up_out, sems.at[1]),
+        pltpu.make_async_copy(down_ref, down_out, sems.at[2]),
     ]
-    second = [
-        pltpu.make_async_copy(mid, dst, sem_out.at[i]) for i, (_, mid, dst) in enumerate(moves)
-    ]
-    for copy in first:
+    for copy in copies:
         copy.start()
     channels = norm_ref.shape[1]
-    norm_out[...] = norm_ref[...]
+    norm_out[...] = norm_ref[0]
     for b in range(2):
         for k in range(3):
             for i in range(taps_ref.shape[1]):
                 taps_out[k, b : b + 1, i * channels : (i + 1) * channels] = taps_ref[
                     b, i, k : k + 1, :
                 ]
-    for copy, after in zip(first, second):
-        copy.wait()
-        after.start()
-    for copy in second:
+    for copy in copies:
         copy.wait()
 
 
 def hand_over(gate_grad, up_grad, down_grad, norms, taps):
     tps, channels = taps.shape[1], taps.shape[3]
-    dma = pltpu.SemaphoreType.DMA
-    big = (gate_grad, up_grad, down_grad)
+    rows = gate_grad.shape[0] - BF16_ROWS
+    f32 = jnp.float32
     return pl.pallas_call(
         hand_over_kernel,
-        out_shape=tuple(jax.ShapeDtypeStruct(a.shape, a.dtype) for a in big)
-        + (
-            jax.ShapeDtypeStruct((1, channels), jnp.float32),
-            jax.ShapeDtypeStruct((3, 2, channels * tps), jnp.float32),
+        out_shape=(
+            jax.ShapeDtypeStruct((rows, channels), gate_grad.dtype),
+            jax.ShapeDtypeStruct((rows, channels), gate_grad.dtype),
+            jax.ShapeDtypeStruct(down_grad.shape, f32),
+            jax.ShapeDtypeStruct((channels,), f32),
+            jax.ShapeDtypeStruct((3, 2, channels * tps), f32),
         ),
         in_specs=[pl.BlockSpec(memory_space=pl.ANY)] * 3
         + [pl.BlockSpec(memory_space=pltpu.VMEM)] * 2,
         out_specs=[pl.BlockSpec(memory_space=pl.ANY)] * 3
         + [pl.BlockSpec(memory_space=pltpu.VMEM)] * 2,
-        scratch_shapes=[pltpu.VMEM(a.shape, a.dtype) for a in big] + [dma((12,)), dma((12,))],
+        scratch_shapes=[pltpu.SemaphoreType.DMA((3,))],
+        compiler_params=pltpu.CompilerParams(vmem_limit_bytes=2_000_000),
         name="hand_over",
-    )(*big, norms, taps)
+    )(gate_grad, up_grad, down_grad, norms, taps)
 
 
 def whole_body(gate_pre, up_pre, gate_taps, up_taps, down_proj, cotangent):
@@ -1152,20 +1113,18 @@
     gate_grad, up_grad, down_grad, norms, taps = pl.pallas_call(
         functools.partial(whole_kernel, chips, tps, scale),
         out_shape=(
-            jax.ShapeDtypeStruct((total, channels), bf16),
-            jax.ShapeDtypeStruct((total, channels), bf16),
-            jax.ShapeDtypeStruct((channels, cols), f32),
-            jax.ShapeDtypeStruct((1, channels), f32),
-            jax.ShapeDtypeStruct((2, tps, 4, channels), f32),
+            pltpu.VMEM((total + BF16_ROWS, channels), bf16),
+            pltpu.VMEM((total + BF16_ROWS, channels), bf16),
+            pltpu.VMEM((channels, cols), f32),
+            pltpu.VMEM((1, channels), f32),
+            pltpu.VMEM((2, tps, 4, channels), f32),
         ),
         in_specs=[
             pl.BlockSpec(memory_space=pl.ANY)
         ]
         * 6,
-        out_specs=[pl.BlockSpec(memory_space=pl.ANY)] * 5,
+        out_specs=[pl.BlockSpec(memory_space=pltpu.VMEM)] * 5,
         scratch_shapes=[
-            pltpu.VMEM((total + BF16_ROWS, channels), bf16),
-            pltpu.VMEM((total + BF16_ROWS, channels), bf16),
             pltpu.VMEM((2, 3, channels), bf16),
             pltpu.VMEM((2, 4, channels), f32),
             pltpu.VMEM((total + 8, channels), f32),
@@ -1185,10 +1144,8 @@
             pltpu.VMEM((2, 4, channels), f32),
             pltpu.VMEM((4, channels), f32),
             pltpu.VMEM((chips, 4, channels), f32),
-            pltpu.VMEM((2, tps, 4, channels), f32),
             pltpu.VMEM((fs, 1, channels), f32),
-            pltpu.VMEM((1, channels), f32),
-            dma((11,)),
+            dma((9,)),
             dma((2, chips, PIECES)),
             dma((2, chips, PIECES)),
             dma((chips, PIECES)),
@@ -1209,7 +1166,6 @@
             dma((2, tps)),
             dma((fs,)),
             dma((fs,)),
-            dma((PIECES,)),
         ],
         compiler_params=pltpu.CompilerParams(
             collective_id=2, has_side_effects=True, vmem_limit_bytes=VMEM_BYTES
@@ -1219,11 +1175,11 @@
     gate_grad, up_grad, down_grad, norms, taps = hand_over(
         gate_grad, up_grad, down_grad, norms, taps
     )
-    return gate_grad, up_grad, down_grad, norms.reshape(channels), taps.transpose(1, 0, 2)
-
-
-VMEM_BYTES = 64_000_000
-SPARE_BYTES = 5_000_000
+    return gate_grad, up_grad, down_grad, norms, taps.transpose(1, 0, 2)
+
+
+VMEM_BYTES = 56_500_000
+SPARE_BYTES = 0
 
 
 def fits_whole(gate_pre, gate_taps, down_proj, cotangent):
@@ -1236,7 +1192,7 @@
     tiled = tiled and channels >= LANES * PIECES and total % ROW_TILE == 0
     tiled = tiled and rows % (2 * BF16_ROWS) == 0 and gate_taps.shape[0] == 3
     tiled = tiled and fs % 2 == 0 and chips % 2 == 0 and chips >= 4 and tps >= 4
-    held = 2 * total * channels * (2 + 4) + total * channels * (2 + 4)
+    held = 2 * total * channels * 4 + total * channels * (2 + 4)
     held += (total + channels) * features * 2 + channels * cols * chips * (5 * 2 + 4)
     return tiled and held + SPARE_BYTES < VMEM_BYTES
 

time: 88.3 us -> 82.6 us (0.935)
  Pallas kernels: 86.1 us -> 81.9 us
  other arithmetic: 1.31 us -> 0 us
    pallas_call x1, Pallas kernels: 7.37 us -> 3.69 us  [hand_over(): pl.pallas_call(hand_over_kernel, out_shape=(jax.ShapeDtypeStruct((rows, c...]
    pallas_call x1 -> x0, other arithmetic: 1.31 us -> none  [hand_over(): pl.pallas_call(hand_over_kernel, out_shape=tuple((jax.ShapeDtypeStruct(a....]
where the time goes in v3:
time: 82.6 us; the launch traced here: 82.5 us
  Pallas kernels  81.9 us (99%)
    pallas_call x1, Pallas kernels, whole_body(): pl.pallas_call(functools.partial(whole_kernel, chips, tps, scale), out_sh...  78.2 us
    pallas_call x1, Pallas kernels, hand_over(): pl.pallas_call(hand_over_kernel, out_shape=(jax.ShapeDtypeStruct((rows, c...  3.69 us

profile of v3, /device:TPU:0, one launch (start us, length us, event | category | flops | bytes accessed | tf_op | source)
XLA Modules:
  0.0 82.5 jit_solution(5378293933084171939)
XLA Ops:
  0.6 78.2 %whole_layer.1 = (bf16[1040,1408]{1,0:T(8,128)(2,1)S(1)}, bf16[1040,1408]{1,0:T(8,128)(2,1)S(1)}, f32[1408,256]{1,0:T(8,128)S(1)}, f32[1,1408]{1,0:T(1,128)S(1)}, f32[2,4,4,1408]{3,2,1,0:T(4,128)S(1)}) custom-call(bf16[1024,1408]{1,0:T(8,128)(2,1)} %gate_ref.1, bf16[1024,1408]{1,0:T(8,128)(2,1)} %up_ref.1, bf16[3,5632]{1,0:T(4,128)(2,1)} %gtaps_ref.1, ...), custom_call_target="tpu_custom_call" | custom-call | tf_op jit(solution)/shard_map/whole_layer/pallas_call | solution.py:1113
  78.8 3.7 %hand_over.1 = (bf16[1024,1408]{1,0:T(8,128)(2,1)}, bf16[1024,1408]{1,0:T(8,128)(2,1)}, f32[1408,256]{1,0:T(8,128)}, f32[1408]{0:T(1024)}, f32[3,2,5632]{2,1,0:T(2,128)}) custom-call(bf16[1040,1408]{1,0:T(8,128)(2,1)S(1)} %get-tuple-element.15.refs_0_, bf16[1040,1408]{1,0:T(8,128)(2,1)S(1)} %get-tuple-element.16.refs_1_, ...), custom_call_target="tpu_custom_call" | custom-call | tf_op jit(solution)/shard_map/hand_over/pallas_call | solution.py:1084

commit v4 on v3

--- a/solution.py
+++ b/solution.py
@@ -403,8 +403,8 @@
 
 
 def cut(channels):
-    tiles = channels // LANES
-    sizes = [(tiles + PIECES - 1 - i) // PIECES * LANES for i in range(PIECES)]
+    tiles, most = channels // LANES - 1, PIECES - 1
+    sizes = [(tiles + most - 1 - i) // most * LANES for i in range(most)] + [LANES]
     return [(sum(sizes[:i]), sizes[i]) for i in range(PIECES)]
 
 
@@ -776,13 +776,13 @@
 
         both_ways(body)
 
-    def pair_down_wait(chip):
-        for s in range(PIECES):
+    def pair_down_wait(chip, one=None):
+        for s in range(PIECES) if one is None else (one,):
             pair_down(chip, 1 - core, s).wait_recv()
 
     last_chip = (1 - half) * (chips - 1)
 
-    def hidden_grad(first_chip, count, add):
+    def hidden_grad(first_chip, count, add, tile_from=0, tile_to=None):
         depth = count * chip_cols
         col = pl.ds(pl.multiple_of(first_chip * chip_cols, chip_cols), depth)
 
@@ -804,9 +804,10 @@
             one(pl.multiple_of(n * wide, wide), wide)
             return carry
 
-        lax.fori_loop(0, channels // wide, step, 0)
-        if channels % wide:
-            one(channels - channels % wide, channels % wide)
+        whole = channels // wide
+        lax.fori_loop(tile_from, whole if tile_to is None else tile_to, step, 0)
+        if channels % wide and tile_to is None:
+            one(whole * wide, channels % wide)
 
     def ring_ends(k):
         for step in range(2, half_ring + 1):
@@ -840,46 +841,29 @@
         for s in range(mid, PIECES):
             slot(p, s)
     ring_step(chips - 1, 1)
+    second_chip = (1 - half) * (chips - 2) + half
+    pair_down_wait(second_chip)
+    hidden_grad(second_chip, 1, False)
     ready(chips - 2)
     for s in range(mid):
         pair_terms_wait(chips - 2, s)
     slot(chips - 2, 0)
     first_sum(chips - 2, 0)
     ready(chips - 1)
-    for i in range(chips - 1):
-        pair_down_wait(half + i)
-    hidden_grad(half, chips - 1, False)
+    for i in range(chips - 2):
+        pair_down_wait(2 * half + i)
+    hidden_grad(2 * half, chips - 2, True)
     for s in range(1, mid):
         first_sum(chips - 2, s)
     for s in range(PIECES):
         pair_terms_wait(chips - 1, s)
     for s in range(1, mid):
         slot(chips - 2, s)
-    for s in range(mid, PIECES):
+    for s in range(mid, PIECES - 1):
         slot(chips - 2, s, send=False)
-    pair_down_wait(last_chip)
-    hidden_grad(last_chip, 1, True)
-
+    for s in range(PIECES - 1):
+        pair_down_wait(last_chip, s)
     edge = 8
-    row_index = lax.broadcasted_iota(jnp.int32, (edge, channels), 0)
-    top = pl.ds(0, edge)
-    edge_send[...] = jnp.where(
-        row_index < 2,
-        hg_v[top, :] * a_v[top, :],
-        pltpu.roll(hg_v[top, :] * b_v[top, :], 2, 0),
-    )
-    edge_copy = remote(
-        edge_send, edge_recv, e_send.at[0], e_recv.at[0], {"fs": (f + fs - 1) % fs}
-    )
-
-    @pl.when(f > 0)
-    def _():
-        edge_copy.start()
-
-    for s in range(mid, PIECES):
-        pair_terms_wait(chips - 2, s)
-        first_sum(chips - 2, s)
-        slot(chips - 2, s, arrive=False)
 
     def grads(start, lane, sums):
         window = pl.ds(start, BLOCK + edge)
@@ -921,8 +905,39 @@
                 tap_mine[b, k : k + 1, lane] = jnp.sum(sums[3 * b + k], axis=0, keepdims=True)
         return carry
 
-    lax.fori_loop(0, lane_tiles // 2, grad_lanes, 0)
-    lax.fori_loop(lane_tiles // 2, lane_tiles, grad_lanes, 0)
+    def grad_range(first, last):
+        lax.fori_loop(first, last, grad_lanes, 0)
+
+    early_tiles = pieces[-1][0] // (2 * LANES)
+    hidden_grad(last_chip, 1, True, 0, early_tiles)
+    grad_range(0, lane_tiles // 4)
+    slot(chips - 2, PIECES - 1, send=False)
+    grad_range(lane_tiles // 4, lane_tiles // 2)
+    pair_down_wait(last_chip, PIECES - 1)
+    hidden_grad(last_chip, 1, True, early_tiles)
+
+    row_index = lax.broadcasted_iota(jnp.int32, (edge, channels), 0)
+    top = pl.ds(0, edge)
+    edge_send[...] = jnp.where(
+        row_index < 2,
+        hg_v[top, :] * a_v[top, :],
+        pltpu.roll(hg_v[top, :] * b_v[top, :], 2, 0),
+    )
+    edge_copy = remote(
+        edge_send, edge_recv, e_send.at[0], e_recv.at[0], {"fs": (f + fs - 1) % fs}
+    )
+
+    @pl.when(f > 0)
+    def _():
+        edge_copy.start()
+
+    for s in range(mid, PIECES):
+        pair_terms_wait(chips - 2, s)
+    for s in range(mid, PIECES - 1):
+        first_sum(chips - 2, s)
+        slot(chips - 2, s, arrive=False)
+
+    grad_range(lane_tiles // 2, lane_tiles)
 
     @pl.when(f < fs - 1)
     def _():
@@ -956,6 +971,8 @@
     tap_chip[z] = tap_mine[core] + tap_pair[...]
     for i in range(1, chips):
         tap_chip_copy(i, z).start()
+    first_sum(chips - 2, PIECES - 1)
+    slot(chips - 2, PIECES - 1, arrive=False)
 
     ones = jnp.ones((8, cols), bf16)
     contract = (((1,), (1,)), ((), ()))

time: 82.6 us -> 82.3 us (level)
  no operation moved by 1% of the time
where the time goes in v4:
time: 82.3 us; the launch traced here: 82.1 us
  Pallas kernels  81.5 us (99%)
    pallas_call x1, Pallas kernels, whole_body(): pl.pallas_call(functools.partial(whole_kernel, chips, tps, scale), out_sh...  77.8 us
    pallas_call x1, Pallas kernels, hand_over(): pl.pallas_call(hand_over_kernel, out_shape=(jax.ShapeDtypeStruct((rows, c...  3.69 us

profile of v4, /device:TPU:0, one launch (start us, length us, event | category | flops | bytes accessed | tf_op | source)
XLA Modules:
  0.0 82.1 jit_solution(14682365119801764401)
XLA Ops:
  0.6 77.8 %whole_layer.1 = (bf16[1040,1408]{1,0:T(8,128)(2,1)S(1)}, bf16[1040,1408]{1,0:T(8,128)(2,1)S(1)}, f32[1408,256]{1,0:T(8,128)S(1)}, f32[1,1408]{1,0:T(1,128)S(1)}, f32[2,4,4,1408]{3,2,1,0:T(4,128)S(1)}) custom-call(bf16[1024,1408]{1,0:T(8,128)(2,1)} %gate_ref.1, bf16[1024,1408]{1,0:T(8,128)(2,1)} %up_ref.1, bf16[3,5632]{1,0:T(4,128)(2,1)} %gtaps_ref.1, ...), custom_call_target="tpu_custom_call" | custom-call | tf_op jit(solution)/shard_map/whole_layer/pallas_call | solution.py:1130
  78.5 3.7 %hand_over.1 = (bf16[1024,1408]{1,0:T(8,128)(2,1)}, bf16[1024,1408]{1,0:T(8,128)(2,1)}, f32[1408,256]{1,0:T(8,128)}, f32[1408]{0:T(1024)}, f32[3,2,5632]{2,1,0:T(2,128)}) custom-call(bf16[1040,1408]{1,0:T(8,128)(2,1)S(1)} %get-tuple-element.15.refs_0_, bf16[1040,1408]{1,0:T(8,128)(2,1)S(1)} %get-tuple-element.16.refs_1_, ...), custom_call_target="tpu_custom_call" | custom-call | tf_op jit(solution)/shard_map/hand_over/pallas_call | solution.py:1101
